TPU v7x, 32 devices: a whole 2x2x4 slice. The times are simulated.
32 devices in a mesh: sp: 8 (over z, x), tp: 4 (over y, core).
Axes of the slice: x: 2, y: 2, z: 4, core: 2. Of those that a mesh axis runs over, the one named last changes fastest.
Arguments:
- moe_input: bfloat16 [2048, 2048], P('sp'), may hold values from -6 to 6
- cotangent: bfloat16 [2048, 2048], P('sp'), may hold values from -6 to 6
- expert_ids: int32 [2048, 2], P('sp'), may hold values from 0 to 7, as said below
- route_weights: float32 [2048, 2], P('sp'), may hold values from 0.05 to 1
- gate_weight: bfloat16 [8, 2048, 1024], P('sp', None, 'tp'), may hold values from -0.125 to 0.125
- up_weight: bfloat16 [8, 2048, 1024], P('sp', None, 'tp'), may hold values from -0.125 to 0.125
- down_weight: bfloat16 [8, 1024, 2048], P('sp', 'tp'), may hold values from -0.1875 to 0.1875
- out_weight: bfloat16 [2048, 1024], P(None, 'tp'), may hold values from -0.1875 to 0.1875
- mixer_out: bfloat16 [2048, 1024], P('sp', 'tp'), may hold values from -6 to 6
- query_vectors: bfloat16 [2048, 512], P('sp', 'tp'), may hold values from -0.62109375 to 0.62109375
- key_vectors: bfloat16 [2048, 512], P('sp', 'tp'), may hold values from -0.62109375 to 0.62109375
- value_vectors: bfloat16 [2048, 1024], P('sp', 'tp'), may hold values from -6 to 6
- log_decay: float32 [2048, 512], P('sp', 'tp'), may hold values from -2 to 0
Outputs:
- grad_gate: bfloat16 [8, 2048, 1024], P('sp', None, 'tp')
- grad_up: bfloat16 [8, 2048, 1024], P('sp', None, 'tp')
- grad_down: bfloat16 [8, 1024, 2048], P('sp', 'tp')
- grad_out_weight: float32 [2048, 1024], P('sp', 'tp')
- grad_queries: bfloat16 [2048, 512], P('sp', 'tp')
- grad_keys: bfloat16 [2048, 512], P('sp', 'tp')
- grad_values: bfloat16 [2048, 1024], P('sp', 'tp')
- grad_log_decay: float32 [2048, 512], P('sp', 'tp')
Inputs may be any that keep to these rules, and one draw needn't show every extreme that they name: `expert_ids`: each row names two different experts of one group, expert e lying in group e // 2. Each aligned block of 256 rows names every expert exactly 64 times and has equally many rows in each of the 4 groups.
All inputs are finite; a program needn't handle non-finite values.
Results may differ from a plain program's by a relative error of at most 0.01145.
Values may be sent and summed in bfloat16 or wider, within the bound.
A program may use at most 64 MiB of HBM per device.

v0:
```python
import jax
import jax.numpy as jnp
from jax import lax
from jax.sharding import PartitionSpec as P

KEY_CHANNELS = 64
VAL_DIM = 128
BLOCK = 64


HIGHEST = lax.Precision.HIGHEST


def entering(shard, axis, combine, identity, reverse):
    devices, place = (lax.axis_size(axis), lax.axis_index(axis))
    everything = jax.tree.map(lambda part: lax.all_gather(part, axis), shard)
    start = jax.tree.map(
        lambda part, zero: jnp.broadcast_to(jnp.asarray(zero, part.dtype), part.shape),
        shard,
        identity,
    )

    def lap(k, before):
        at = devices - 1 - k if reverse else k
        reached = at > place if reverse else at < place
        new = combine(before, jax.tree.map(lambda part: part[at], everything))
        return jax.tree.map(lambda a, b: jnp.where(reached, a, b), new, before)

    return lax.fori_loop(0, devices, lap, start)


def block_step(memory, inputs):
    query_block, key_block, value_block, decay_block = inputs
    block_len = query_block.shape[1]
    causal = jnp.tril(jnp.ones((block_len, block_len), dtype=bool))
    cumulative = jnp.cumsum(decay_block, axis=1)
    carried = jnp.einsum(
        "hcd,hdv->hcv", query_block * jnp.exp(cumulative), memory, precision=HIGHEST
    )
    difference = cumulative[:, :, None, :] - cumulative[:, None, :, :]
    decay = jnp.exp(jnp.where(causal[None, :, :, None], difference, -jnp.inf))
    scores = jnp.einsum("htd,hsd,htsd->hts", query_block, key_block, decay, precision=HIGHEST)
    within = jnp.einsum("hts,hsv->htv", scores, value_block, precision=HIGHEST)
    final_row = cumulative[:, -1:, :]
    memory = jnp.exp(final_row[:, 0, :])[:, :, None] * memory + jnp.einsum(
        "hsd,hsv->hdv", key_block * jnp.exp(final_row - cumulative), value_block, precision=HIGHEST
    )
    return (memory, carried + within)


def run_blocks(query_heads, key_heads, value_heads, decay_heads, memory):
    head_count = query_heads.shape[0]
    length = query_heads.shape[1]
    block_count = length // BLOCK

    def to_blocks(matrix):
        return matrix.reshape(head_count, block_count, BLOCK, matrix.shape[-1]).transpose(
            1, 0, 2, 3
        )

    memory, outputs = lax.scan(
        jax.checkpoint(block_step),
        memory,
        (
            to_blocks(query_heads),
            to_blocks(key_heads),
            to_blocks(value_heads),
            to_blocks(decay_heads),
        ),
    )
    return (outputs.transpose(1, 0, 2, 3).reshape(head_count, length, outputs.shape[-1]), memory)


def chain_combine(former, latter):
    return (former[0] * latter[0], latter[1] + latter[0][:, :, None] * former[1])


def expert_pass(routed, routed_cot, gate_local, up_local, down_local):
    pre_gate = jnp.dot(routed, gate_local, preferred_element_type=jnp.float32)
    pre_up = jnp.dot(routed, up_local, preferred_element_type=jnp.float32)
    sigmoid_gate = jax.nn.sigmoid(pre_gate)
    activated = pre_gate * sigmoid_gate
    hidden = (activated * pre_up).astype(jnp.bfloat16)
    delta_hidden = jnp.dot(routed_cot, down_local.T, preferred_element_type=jnp.float32)
    grad_down = jnp.dot(hidden.T, routed_cot, preferred_element_type=jnp.float32).astype(
        jnp.bfloat16
    )
    delta_gate = (
        delta_hidden * pre_up * sigmoid_gate * (1.0 + pre_gate * (1.0 - sigmoid_gate))
    ).astype(jnp.bfloat16)
    delta_up = (delta_hidden * activated).astype(jnp.bfloat16)
    grad_gate = jnp.dot(routed.T, delta_gate, preferred_element_type=jnp.float32).astype(
        jnp.bfloat16
    )
    grad_up = jnp.dot(routed.T, delta_up, preferred_element_type=jnp.float32).astype(jnp.bfloat16)
    partial_value = jnp.dot(delta_gate, gate_local.T, preferred_element_type=jnp.float32)
    partial_value = partial_value + jnp.dot(
        delta_up, up_local.T, preferred_element_type=jnp.float32
    )
    return (grad_gate, grad_up, grad_down, partial_value)


def mixer_backward(query_vectors, key_vectors, value_vectors, log_decay, delta_mixer):
    tok_count = query_vectors.shape[0]

    def heads_first(matrix, channel_size):
        return matrix.astype(jnp.float32).reshape(tok_count, -1, channel_size).transpose(1, 0, 2)

    def tokens_first(matrix):
        return matrix.transpose(1, 0, 2).reshape(tok_count, -1)

    query_heads = heads_first(query_vectors, KEY_CHANNELS)
    key_heads = heads_first(key_vectors, KEY_CHANNELS)
    value_heads = heads_first(value_vectors, VAL_DIM)
    decay_heads = heads_first(log_decay, KEY_CHANNELS)
    cot_heads = heads_first(delta_mixer, VAL_DIM)
    cumulative = jnp.cumsum(decay_heads, axis=1)
    decay_total = cumulative[:, -1, :]
    retention = jnp.exp(decay_total)
    local_state = jnp.einsum(
        "hld,hlv->hdv",
        key_heads * jnp.exp(decay_total[:, None, :] - cumulative),
        value_heads,
        precision=HIGHEST,
    )
    local_pull = jnp.einsum(
        "hld,hlv->hdv",
        query_heads * KEY_CHANNELS ** (-0.5) * jnp.exp(cumulative),
        cot_heads,
        precision=HIGHEST,
    )
    identity = (jnp.ones_like(retention), jnp.zeros_like(local_state))
    start_state = entering((retention, local_state), "sp", chain_combine, identity, False)[1]
    end_pull = entering((retention, local_pull), "sp", chain_combine, identity, True)[1]

    def local_forward(query_in, key_in, value_in, decay_in):
        return run_blocks(
            query_in * KEY_CHANNELS ** (-0.5), key_in, value_in, decay_in, start_state
        )

    pullback = jax.vjp(local_forward, query_heads, key_heads, value_heads, decay_heads)[1]
    grads = pullback((cot_heads, end_pull))
    return (
        tokens_first(grads[0]).astype(jnp.bfloat16),
        tokens_first(grads[1]).astype(jnp.bfloat16),
        tokens_first(grads[2]).astype(jnp.bfloat16),
        tokens_first(grads[3]),
    )


def shards(
    moe_input,
    cotangent,
    expert_ids,
    route_weights,
    gate_weight,
    up_weight,
    down_weight,
    out_weight,
    mixer_out,
    query_vectors,
    key_vectors,
    value_vectors,
    log_decay,
):
    tok_count = moe_input.shape[0]
    model_width = moe_input.shape[1]
    slot_total = 2 * tok_count
    flat_ids = expert_ids.reshape(-1)
    sorting = jnp.argsort(flat_ids, stable=True)
    source_rows = sorting // 2
    inverse = jnp.argsort(sorting)
    gate_local = gate_weight[0]
    up_local = up_weight[0]
    down_local = down_weight[0]
    quarter = model_width // lax.axis_size("tp")
    offset = lax.axis_index("tp") * quarter
    own_input = lax.dynamic_slice_in_dim(moe_input, offset, quarter, 1)
    own_cot = lax.dynamic_slice_in_dim(cotangent, offset, quarter, 1)
    own_scaled = (route_weights[:, :, None] * own_cot[:, None, :].astype(jnp.float32)).astype(
        jnp.bfloat16
    )
    own_scaled = own_scaled.reshape(slot_total, quarter)
    arrived = (
        lax.all_to_all(own_input[source_rows], "sp", split_axis=0, concat_axis=0, tiled=True),
        lax.all_to_all(own_scaled[sorting], "sp", split_axis=0, concat_axis=0, tiled=True),
    )
    routed, routed_cot = (
        lax.all_gather(arrived[0], "tp", axis=1, tiled=True),
        lax.all_gather(arrived[1], "tp", axis=1, tiled=True),
    )
    grad_gate, grad_up, grad_down, partial_value = expert_pass(
        routed, routed_cot, gate_local, up_local, down_local
    )
    summed = lax.psum_scatter(
        partial_value.astype(jnp.bfloat16), "tp", scatter_dimension=1, tiled=True
    )
    returned = lax.all_to_all(summed, "sp", split_axis=0, concat_axis=0, tiled=True)
    per_slot = returned[inverse].reshape(tok_count, 2, quarter).astype(jnp.float32)
    own_grad = (own_cot.astype(jnp.float32) + per_slot[:, 0] + per_slot[:, 1]).astype(jnp.bfloat16)
    token_grad = lax.all_gather(own_grad, "tp", axis=1, tiled=True)
    delta_mixer = jnp.dot(token_grad, out_weight, preferred_element_type=jnp.float32).astype(
        jnp.bfloat16
    )
    grad_out_weight = lax.psum_scatter(
        jnp.dot(token_grad.T, mixer_out, preferred_element_type=jnp.float32),
        "sp",
        scatter_dimension=0,
        tiled=True,
    )
    gradients = mixer_backward(query_vectors, key_vectors, value_vectors, log_decay, delta_mixer)
    return (
        grad_gate[None],
        grad_up[None],
        grad_down[None],
        grad_out_weight,
        gradients[0],
        gradients[1],
        gradients[2],
        gradients[3],
    )


def solution(mesh):
    return jax.shard_map(
        shards,
        mesh=mesh,
        in_specs=(
            P("sp", None),
            P("sp", None),
            P("sp", None),
            P("sp", None),
            P("sp", None, "tp"),
            P("sp", None, "tp"),
            P("sp", "tp", None),
            P(None, "tp"),
            P("sp", "tp"),
            P("sp", "tp"),
            P("sp", "tp"),
            P("sp", "tp"),
            P("sp", "tp"),
        ),
        out_specs=(
            P("sp", None, "tp"),
            P("sp", None, "tp"),
            P("sp", "tp", None),
            P("sp", "tp"),
            P("sp", "tp"),
            P("sp", "tp"),
            P("sp", "tp"),
            P("sp", "tp"),
        ),
        check_vma=False,
    )
```

profile of v0, /device:TPU:10, one launch (start us, length us, event | category | flops | bytes accessed | tf_op | source)
XLA Modules:
  0.0 282.4 jit_solution(11970388747778692487)
XLA Ops:
  7.2 0.9 copy.179
  8.3 3.8 %sort.34 = (s32[512]{0:T(512)}, s32[512]{0:T(512)S(1)}) sort(s32[512]{0:T(512)S(1)} %reshape.170, s32[512]{0:T(512)S(1)} %iota.42), dimensions={0}, to_apply=%region_0.0 | sort | flops 4608 | bytes 8192 | tf_op jit(solution)/shard_map/jit(argsort)/sort | solution.py:170
  12.1 1.1 dynamic-slice_convert_fusion
  13.2 2.0 gather_fusion
  15.2 18.5 %all_to_all.36 = bf16[8,64,512]{2,1,0:T(8,128)(2,1)} all-to-all(bf16[8,64,512]{2,1,0:T(8,128)(2,1)S(1)} %bitcast.315), channel_id=1, replica_groups=mesh['sp'=8,'tp'=4] {'sp'}, dimensions={0} | all-to-all | bytes 1048576 | tf_op jit(solution)/shard_map/all_to_all | solution.py:185
  34.1 0.7 mul.256
  35.2 2.0 gather_fusion.1
  37.2 17.9 %all_to_all.37 = bf16[8,64,512]{2,1,0:T(8,128)(2,1)} all-to-all(bf16[8,64,512]{2,1,0:T(8,128)(2,1)S(1)} %bitcast.316), channel_id=1, replica_groups=mesh['sp'=8,'tp'=4] {'sp'}, dimensions={0} | all-to-all | bytes 1048576 | tf_op jit(solution)/shard_map/all_to_all | solution.py:186
  55.2 1.9 all-gather.7.cloned.1.call-done
  57.1 2.3 fusion.32
  59.4 2.5 fusion.35
  61.9 19.3 %all-gather.9.cloned.1.call-done = bf16[512,2048]{1,0:T(8,128)(2,1)} async-done(((bf16[512,512]{1,0:T(8,128)(2,1)}), bf16[512,2048]{1,0:T(8,128)(2,1)}) %all-gather.9.cloned.1.call-update) | async-done | bytes 2097168 | tf_op jit(solution)/shard_map/all_gather | solution.py:190
  81.2 2.7 multiply_convert_fusion.2
  83.9 0.7 copy-done.12
  84.6 0.7 fusion.30
  85.4 2.1 add_convert_fusion
  87.9 1.2 reduce-window.6
  90.1 14.2 %all-gather.1 = f32[16,1,64]{2,1,0:T(1,128)S(1)} all-gather(f32[2,1,64]{2,1,0:T(1,128)S(1)} %bitcast.346), channel_id=3, replica_groups=mesh['sp'=8,'tp'=4] {'sp'}, dimensions={0}, use_global_device_ids=true | all-gather | bytes 4608 | tf_op jit(solution)/shard_map/all_gather | solution.py:16
  105.0 31.2 %all-gather.2 = f32[16,64,128]{2,1,0:T(8,128)S(1)} all-gather(f32[2,64,128]{2,1,0:T(8,128)S(1)} %fusion.43), channel_id=4, replica_groups=mesh['sp'=8,'tp'=4] {'sp'}, dimensions={0}, use_global_device_ids=true | all-gather | bytes 589824 | tf_op jit(solution)/shard_map/all_gather | solution.py:16
  136.2 10.6 %all-to-all-start.2 = ((bf16[8,64,512]{2,1,0:T(8,128)(2,1)}), bf16[8,64,512]{2,1,0:T(8,128)(2,1)S(1)}, u32[]{:S(2)}, u32[]{:S(2)}) async-start(bf16[8,64,512]{2,1,0:T(8,128)(2,1)} %bitcast.335), calls=%async_computation.3 | async-start | bytes 1048576 | tf_op jit(solution)/shard_map/all_to_all | solution.py:198
  146.8 1.1 while.67
  148.1 3.8 %sort.35 = (s32[512]{0:T(512)}, s32[512]{0:T(512)S(1)}) sort(s32[512]{0:T(512)S(1)} %get-tuple-element.514, s32[512]{0:T(512)S(1)} %iota.43), dimensions={0}, to_apply=%region_2.3 | sort | flops 4608 | bytes 8192 | tf_op jit(solution)/shard_map/jit(argsort)/sort | solution.py:172
  152.4 2.9 %all-to-all-done.2 = bf16[8,64,512]{2,1,0:T(8,128)(2,1)S(1)} async-done(((bf16[8,64,512]{2,1,0:T(8,128)(2,1)}), bf16[8,64,512]{2,1,0:T(8,128)(2,1)S(1)}, u32[]{:S(2)}, u32[]{:S(2)}) %all-to-all-start.2) | async-done | bytes 524320 | tf_op jit(solution)/shard_map/all_to_all | solution.py:198
  155.3 2.6 gather_fusion.2
  157.9 1.7 reshape.184
  159.6 0.8 fusion.53
  160.4 1.9 fusion.40
  162.3 5.1 %while.64 = (s32[]{:T(128)}, f32[2,64,128]{2,1,0:T(8,128)S(1)}, f32[4,2,64,128]{3,2,1,0:T(8,128)}, f32[4,2,64,64]{3,2,1,0:T(8,128)S(1)}, f32[4,2,64,64]{2,0,3,1:...) while((s32[]{:T(128)}, f32[2,64,128]{2,1,0:T(8,128)S(1)}, ...), condition=%wide.region_12.13_spmd, body=%wide.region_10.12_spmd.sunk | while | flops 13148162 | bytes 725105 | solution.py:61
  162.4 0.6 bitcast_dynamic-update-slice_fusion.5
  164.9 0.6 bitcast_dynamic-update-slice_fusion.5
  167.6 0.7 broadcast_convert_fusion
  168.3 3.4 %fusion.27 = bf16[1,2048,256]{2,1,0:T(8,128)(2,1)} fusion(bf16[512,2048]{1,0:T(8,128)(2,1)} %all-gather.7.cloned.1.call-done, bf16[512,256]{1,0:T(8,128)(2,1)S(1)} %copy-done.13), kind=kOutput, calls=%fused_computation.70 | convolution fusion | flops 537395200 | bytes 3407872 | tf_op jit(solution)/shard_map/dot_general | solution.py:92
  171.7 2.8 %fusion.28 = bf16[1,2048,256]{2,1,0:T(8,128)(2,1)} fusion(bf16[512,2048]{1,0:T(8,128)(2,1)S(1)} %copy-done.20, bf16[512,256]{1,0:T(8,128)(2,1)} %copy-done.14), kind=kOutput, calls=%fused_computation.71 | convolution fusion | flops 537395200 | bytes 3407872 | tf_op jit(solution)/shard_map/dot_general | solution.py:95
  174.6 1.8 fusion.29
  176.4 2.3 all-gather.11.cloned.1.call-done
  178.6 3.1 %fusion.57 = f32[2048,256]{1,0:T(8,128)} fusion(bf16[256,2048]{1,0:T(8,128)(2,1)} %all-gather.11.cloned.1.call-done, bf16[256,256]{1,0:T(8,128)(2,1)} %param.29), kind=kOutput, calls=%fused_computation.131 | convolution fusion | flops 268435456 | bytes 3276800 | tf_op jit(solution)/shard_map/dot_general | solution.py:206
  181.8 2.4 convolution_convert_fusion.3
  184.2 1.0 copy.189
  185.6 30.0 %all-gather = f32[16,64,128]{2,1,0:T(8,128)S(1)} all-gather(f32[2,64,128]{2,1,0:T(8,128)S(1)} %fusion.45), channel_id=2, replica_groups=mesh['sp'=8,'tp'=4] {'sp'}, dimensions={0}, use_global_device_ids=true | all-gather | bytes 589824 | tf_op jit(solution)/shard_map/all_gather | solution.py:16
  215.7 1.2 while.66
  216.9 0.7 broadcast.54.clone
  217.6 52.6 %while.65 = (s32[]{:T(128)}, f32[2,64,128]{2,1,0:T(8,128)S(1)}, f32[4,2,64,64]{3,1,2,0:T(2,128)S(1)}, bf16[4,2,64,64]{3,1,2,0:T(2,128)(2,1)}, bf16[4,2,64,128]{3...) while((s32[]{:T(128)}, f32[2,64,128]{2,1,0:T(8,128)S(1)}, ...), condition=%wide.region_20.21_spmd, body=%wide.region_13.20_spmd.sunk | while | flops 87216128 | bytes 5496629 | solution.py:61
  217.6 0.9 dynamic-slice_bitcast_fusion.14
  219.9 4.1 %fusion.124 = (f32[2,64,64]{2,1,0:T(8,128)S(1)}, f32[2,64,64]{2,1,0:T(8,128)S(1)}, f32[2,64,64]{2,1,0:T(8,128)S(1)}) fusion(f32[2,64,64]{1,2,0:T(8,128)S(1)} %copy.335, f32[2,64,64]{1,2,0:T(8,128)S(1)} %copy.336, f32[2,64,64]{2,1,0:T(8,128)S(1)} %reduce_window_sum.59, f32[2,64,64]{2,1,0:T(8,128)S(1)} %fusion.123, ...), kind=kLoop, calls=%fused_computation.32.clone.1 | loop fusion | flops 5218304 | bytes 233472 | tf_op jit(solution)/shard_map/transpose(jvp())/while/body/eval_jaxpr/checkpoint/reduce_sum | solution.py:40
  224.9 2.0 fusion.131
  226.9 2.0 fusion.132
  230.8 0.9 dynamic-slice_bitcast_fusion.14
  233.1 4.1 %fusion.124 = (f32[2,64,64]{2,1,0:T(8,128)S(1)}, f32[2,64,64]{2,1,0:T(8,128)S(1)}, f32[2,64,64]{2,1,0:T(8,128)S(1)}) fusion(f32[2,64,64]{1,2,0:T(8,128)S(1)} %copy.335, f32[2,64,64]{1,2,0:T(8,128)S(1)} %copy.336, f32[2,64,64]{2,1,0:T(8,128)S(1)} %reduce_window_sum.59, f32[2,64,64]{2,1,0:T(8,128)S(1)} %fusion.123, ...), kind=kLoop, calls=%fused_computation.32.clone.1 | loop fusion | flops 5218304 | bytes 233472 | tf_op jit(solution)/shard_map/transpose(jvp())/while/body/eval_jaxpr/checkpoint/reduce_sum | solution.py:40
  238.1 2.0 fusion.131
  240.0 2.0 fusion.132
  244.0 0.9 dynamic-slice_bitcast_fusion.14
  246.2 4.1 %fusion.124 = (f32[2,64,64]{2,1,0:T(8,128)S(1)}, f32[2,64,64]{2,1,0:T(8,128)S(1)}, f32[2,64,64]{2,1,0:T(8,128)S(1)}) fusion(f32[2,64,64]{1,2,0:T(8,128)S(1)} %copy.335, f32[2,64,64]{1,2,0:T(8,128)S(1)} %copy.336, f32[2,64,64]{2,1,0:T(8,128)S(1)} %reduce_window_sum.59, f32[2,64,64]{2,1,0:T(8,128)S(1)} %fusion.123, ...), kind=kLoop, calls=%fused_computation.32.clone.1 | loop fusion | flops 5218304 | bytes 233472 | tf_op jit(solution)/shard_map/transpose(jvp())/while/body/eval_jaxpr/checkpoint/reduce_sum | solution.py:40
  251.2 2.0 fusion.131
  253.2 2.0 fusion.132
  257.1 0.9 dynamic-slice_bitcast_fusion.14
  259.4 4.1 %fusion.124 = (f32[2,64,64]{2,1,0:T(8,128)S(1)}, f32[2,64,64]{2,1,0:T(8,128)S(1)}, f32[2,64,64]{2,1,0:T(8,128)S(1)}) fusion(f32[2,64,64]{1,2,0:T(8,128)S(1)} %copy.335, f32[2,64,64]{1,2,0:T(8,128)S(1)} %copy.336, f32[2,64,64]{2,1,0:T(8,128)S(1)} %reduce_window_sum.59, f32[2,64,64]{2,1,0:T(8,128)S(1)} %fusion.123, ...), kind=kLoop, calls=%fused_computation.32.clone.1 | loop fusion | flops 5218304 | bytes 233472 | tf_op jit(solution)/shard_map/transpose(jvp())/while/body/eval_jaxpr/checkpoint/reduce_sum | solution.py:40
  264.4 2.0 fusion.131
  266.4 2.0 fusion.132
  270.5 0.7 copy.214
  271.2 1.0 copy.247
  272.2 0.7 copy.215
  273.0 1.0 copy.212
  274.0 0.8 copy.216
  275.1 0.8 copy.217
  (287 shorter events, 26.3 us)
Async XLA Ops:
  7.2 49.9 %copy-start = (bf16[1,2048,256]{2,1,0:T(8,128)(2,1)S(1)}, bf16[1,2048,256]{2,1,0:T(8,128)(2,1)}, u32[]{:S(2)}) copy-start(bf16[1,2048,256]{2,1,0:T(8,128)(2,1)} %param.25) | copy-start | bytes 3145732
  7.2 49.9 %all-gather.7.cloned.1.call-start = ((), (), s32[]{:S(2)}) async-start(), calls=%async_computation.5 | async-start | bytes 2621440 | tf_op jit(solution)/shard_map/all_gather | solution.py:189
  13.2 21.6 %copy-start.19 = (f32[256,2]{0,1:T(2,128)S(1)}, f32[256,2]{0,1:T(2,128)}, u32[]{:S(2)}) copy-start(f32[256,2]{0,1:T(2,128)} %param.24) | copy-start | bytes 6148
  33.7 47.6 %all-gather.9.cloned.1.call-start = ((), (), s32[]{:S(2)}) async-start(), calls=%async_computation.6 | async-start | bytes 2621440 | tf_op jit(solution)/shard_map/all_gather | solution.py:190
  37.2 22.2 %copy-start.3 = (bf16[1,2048,256]{2,1,0:T(8,128)(2,1)S(1)}, bf16[1,2048,256]{2,1,0:T(8,128)(2,1)}, u32[]{:S(2)}) copy-start(bf16[1,2048,256]{2,1,0:T(8,128)(2,1)} %param.26) | copy-start | bytes 3145732
  55.1 81.1 %reduce-scatter.3.cloned.1.call-start = ((), (), s32[]{:S(2)}) async-start(), calls=%async_computation.7 | async-start | bytes 2621440 | tf_op jit(solution)/shard_map/reduce_scatter | solution.py:195
  59.4 24.5 %copy-start.8 = (f32[512,256]{1,0:T(8,128)}, f32[512,256]{1,0:T(8,128)S(1)}, u32[]{:S(2)}) copy-start(f32[512,256]{1,0:T(8,128)S(1)} %fusion.32) | copy-start | bytes 1572868
  61.9 23.5 %copy-start.10 = (f32[512,256]{1,0:T(8,128)}, f32[512,256]{1,0:T(8,128)S(1)}, u32[]{:S(2)}) copy-start(f32[512,256]{1,0:T(8,128)S(1)} %fusion.35) | copy-start | bytes 1572868
  83.9 0.7 copy-start.12
  83.9 1.4 copy-start.14
  85.4 2.2 copy-start.17
  85.4 2.4 copy-start.15
  85.4 4.2 %copy-start.18 = (bf16[256,128]{1,0:T(8,128)(2,1)S(1)}, bf16[256,128]{1,0:T(8,128)(2,1)}, u32[]{:S(2)}) copy-start(bf16[256,128]{1,0:T(8,128)(2,1)} %param.30) | copy-start | bytes 196612
  87.5 2.4 copy-start.16
  136.2 19.1 %all-to-all-start.2 = ((bf16[8,64,512]{2,1,0:T(8,128)(2,1)}), bf16[8,64,512]{2,1,0:T(8,128)(2,1)S(1)}, u32[]{:S(2)}, u32[]{:S(2)}) async-start(bf16[8,64,512]{2,1,0:T(8,128)(2,1)} %bitcast.335), calls=%async_computation.3 | async-start | bytes 1048576 | tf_op jit(solution)/shard_map/all_to_all | solution.py:198
  146.8 31.8 %all-gather.11.cloned.1.call-start = ((), (), s32[]{:S(2)}) async-start(), calls=%async_computation.8 | async-start | bytes 1310720 | tf_op jit(solution)/shard_map/all_gather | solution.py:201
  160.4 7.9 %copy-start.13 = (bf16[512,256]{1,0:T(8,128)(2,1)S(1)}, bf16[512,256]{1,0:T(8,128)(2,1)}, u32[]{:S(2)}) copy-start(bf16[512,256]{1,0:T(8,128)(2,1)} %copy-done.12) | copy-start | bytes 786436
  162.3 113.6 %reduce-scatter.5.cloned.1.call-start = ((), (), s32[]{:S(2)}) async-start(), calls=%async_computation.9 | async-start | bytes 2359296 | tf_op jit(solution)/shard_map/reduce_scatter | solution.py:205
  167.6 4.2 %copy-start.20 = (bf16[512,2048]{1,0:T(8,128)(2,1)S(1)}, bf16[512,2048]{1,0:T(8,128)(2,1)}, u32[]{:S(2)}) copy-start(bf16[512,2048]{1,0:T(8,128)(2,1)} %all-gather.7.cloned.1.call-done) | copy-start | bytes 6291460
  171.7 2.9 %copy-start.2 = (bf16[512,2048]{1,0:T(8,128)(2,1)S(1)}, bf16[512,2048]{1,0:T(8,128)(2,1)}, u32[]{:S(2)}) copy-start(bf16[512,2048]{1,0:T(8,128)(2,1)} %all-gather.9.cloned.1.call-done) | copy-start | bytes 6291460
  171.7 2.9 %copy-start.9 = (f32[512,256]{1,0:T(8,128)S(1)}, f32[512,256]{1,0:T(8,128)}, u32[]{:S(2)}) copy-start(f32[512,256]{1,0:T(8,128)} %copy-done.8) | copy-start | bytes 1572868
  171.7 2.9 %copy-start.11 = (f32[512,256]{1,0:T(8,128)S(1)}, f32[512,256]{1,0:T(8,128)}, u32[]{:S(2)}) copy-start(f32[512,256]{1,0:T(8,128)} %copy-done.10) | copy-start | bytes 1572868
  178.6 3.2 %copy-start.1 = (bf16[256,2048]{1,0:T(8,128)(2,1)S(1)}, bf16[256,2048]{1,0:T(8,128)(2,1)}, u32[]{:S(2)}) copy-start(bf16[256,2048]{1,0:T(8,128)(2,1)} %all-gather.11.cloned.1.call-done) | copy-start | bytes 3145732
  219.0 9.9 %copy-start.4 = (bf16[4,2,64,64]{3,1,2,0:T(2,128)(2,1)S(1)}, bf16[4,2,64,64]{3,1,2,0:T(2,128)(2,1)}, u32[]{:S(2)}) copy-start(bf16[4,2,64,64]{3,1,2,0:T(2,128)(2,1)} %get-tuple-element.1077) | copy-start | bytes 196612 | tf_op jit(solution)/shard_map/transpose(jvp())/while
  219.0 10.2 %copy-start.6 = (bf16[4,2,64,128]{3,2,0,1:T(8,128)(2,1)S(1)}, bf16[4,2,64,128]{3,2,0,1:T(8,128)(2,1)}, u32[]{:S(2)}) copy-start(bf16[4,2,64,128]{3,2,0,1:T(8,128)(2,1)} %get-tuple-element.1078) | copy-start | bytes 393220 | tf_op jit(solution)/shard_map/transpose(jvp())/while
  229.2 0.7 copy-start.5
  229.5 0.7 copy-start.7
  232.1 9.9 %copy-start.4 = (bf16[4,2,64,64]{3,1,2,0:T(2,128)(2,1)S(1)}, bf16[4,2,64,64]{3,1,2,0:T(2,128)(2,1)}, u32[]{:S(2)}) copy-start(bf16[4,2,64,64]{3,1,2,0:T(2,128)(2,1)} %get-tuple-element.1077) | copy-start | bytes 196612 | tf_op jit(solution)/shard_map/transpose(jvp())/while
  232.2 10.2 %copy-start.6 = (bf16[4,2,64,128]{3,2,0,1:T(8,128)(2,1)S(1)}, bf16[4,2,64,128]{3,2,0,1:T(8,128)(2,1)}, u32[]{:S(2)}) copy-start(bf16[4,2,64,128]{3,2,0,1:T(8,128)(2,1)} %get-tuple-element.1078) | copy-start | bytes 393220 | tf_op jit(solution)/shard_map/transpose(jvp())/while
  242.3 0.7 copy-start.5
  242.7 0.7 copy-start.7
  245.3 9.9 %copy-start.4 = (bf16[4,2,64,64]{3,1,2,0:T(2,128)(2,1)S(1)}, bf16[4,2,64,64]{3,1,2,0:T(2,128)(2,1)}, u32[]{:S(2)}) copy-start(bf16[4,2,64,64]{3,1,2,0:T(2,128)(2,1)} %get-tuple-element.1077) | copy-start | bytes 196612 | tf_op jit(solution)/shard_map/transpose(jvp())/while
  245.3 10.2 %copy-start.6 = (bf16[4,2,64,128]{3,2,0,1:T(8,128)(2,1)S(1)}, bf16[4,2,64,128]{3,2,0,1:T(8,128)(2,1)}, u32[]{:S(2)}) copy-start(bf16[4,2,64,128]{3,2,0,1:T(8,128)(2,1)} %get-tuple-element.1078) | copy-start | bytes 393220 | tf_op jit(solution)/shard_map/transpose(jvp())/while
  255.5 0.7 copy-start.5
  255.8 0.7 copy-start.7
  258.5 9.9 %copy-start.4 = (bf16[4,2,64,64]{3,1,2,0:T(2,128)(2,1)S(1)}, bf16[4,2,64,64]{3,1,2,0:T(2,128)(2,1)}, u32[]{:S(2)}) copy-start(bf16[4,2,64,64]{3,1,2,0:T(2,128)(2,1)} %get-tuple-element.1077) | copy-start | bytes 196612 | tf_op jit(solution)/shard_map/transpose(jvp())/while
  258.5 10.2 %copy-start.6 = (bf16[4,2,64,128]{3,2,0,1:T(8,128)(2,1)S(1)}, bf16[4,2,64,128]{3,2,0,1:T(8,128)(2,1)}, u32[]{:S(2)}) copy-start(bf16[4,2,64,128]{3,2,0,1:T(8,128)(2,1)} %get-tuple-element.1078) | copy-start | bytes 393220 | tf_op jit(solution)/shard_map/transpose(jvp())/while
  268.7 0.7 copy-start.5
  269.0 0.7 copy-start.7
Sparse Core Ops, SparseCore 0:
  33.8 23.2 all-gather.6
  58.6 22.5 all-gather.8
  87.7 31.1 reduce-scatter.2
  162.4 16.1 all-gather.10
  182.6 70.0 reduce-scatter.4
where the time goes:
time: 287 us; the launch traced here: 282 us
  blocking collectives  112 us (39%)
  other arithmetic  53.2 us (19%)
  local copies, waits for them, and re-layouts  32.3 us (11%)
  matrix products  31.8 us (11%)
  waiting for transfers between devices  26.5 us (9%)
  between operations  14.4 us (5%)
  starting transfers between devices  10.8 us (4%)
    all_gather x3, blocking collectives, entering(): everything = jax.tree.map(lambda part: lax.all_gather(part, axis), shard)  75.4 us
    all_gather x1, waiting for transfers between devices, shards(): lax.all_gather(arrived[1], 'tp', axis=1, tiled=True)  19.3 us
    all_to_all x1, blocking collectives, shards(): lax.all_to_all(own_input[source_rows], 'sp', split_axis=0, concat_axis=0,...  18.5 us
    all_to_all x1, blocking collectives, shards(): lax.all_to_all(own_scaled[sorting], 'sp', split_axis=0, concat_axis=0, ti...  17.9 us
    reduce_sum x4, other arithmetic, block_step(): difference = cumulative[:, :, None, :] - cumulative[:, None, :, :]  16.3 us
    while x8, other arithmetic  16 us
    all_to_all x1, starting transfers between devices, shards(): lax.all_to_all(summed, 'sp', split_axis=0, concat_axis=0, tiled=True)  10.6 us
  transfers between devices with their start and end apart: 6, of which 4 were waited for; matrix products, arithmetic and copies ran while one was open for 32% of the time, Pallas kernels for 0%

commit v1 on v0

v1 whole, which is shorter than its diff:
```python
import functools
import jax
import jax.numpy as jnp
from jax import lax
from jax.experimental import pallas as pl
from jax.experimental.pallas import tpu as pltpu
from jax.sharding import PartitionSpec as P

KEY_CHANNELS = 64
VAL_DIM = 128
BLOCK = 64
HIGHEST = lax.Precision.HIGHEST
F32 = jnp.float32
BF16 = jnp.bfloat16


def mm(a, b, ca=1, cb=0, precision=None):
    return lax.dot_general(
        a, b, (((ca,), (cb,)), ((), ())), precision=precision, preferred_element_type=F32
    )


def expert_pass(routed, routed_cot, gate_local, up_local, down_local):
    pre_gate = jnp.dot(routed, gate_local, preferred_element_type=jnp.float32)
    pre_up = jnp.dot(routed, up_local, preferred_element_type=jnp.float32)
    sigmoid_gate = jax.nn.sigmoid(pre_gate)
    activated = pre_gate * sigmoid_gate
    hidden = (activated * pre_up).astype(jnp.bfloat16)
    delta_hidden = jnp.dot(routed_cot, down_local.T, preferred_element_type=jnp.float32)
    grad_down = jnp.dot(hidden.T, routed_cot, preferred_element_type=jnp.float32).astype(
        jnp.bfloat16
    )
    delta_gate = (
        delta_hidden * pre_up * sigmoid_gate * (1.0 + pre_gate * (1.0 - sigmoid_gate))
    ).astype(jnp.bfloat16)
    delta_up = (delta_hidden * activated).astype(jnp.bfloat16)
    grad_gate = jnp.dot(routed.T, delta_gate, preferred_element_type=jnp.float32).astype(
        jnp.bfloat16
    )
    grad_up = jnp.dot(routed.T, delta_up, preferred_element_type=jnp.float32).astype(jnp.bfloat16)
    partial_value = jnp.dot(delta_gate, gate_local.T, preferred_element_type=jnp.float32)
    partial_value = partial_value + jnp.dot(
        delta_up, up_local.T, preferred_element_type=jnp.float32
    )
    return (grad_gate, grad_up, grad_down, partial_value)


def greet(n, axis):
    me = lax.axis_index(axis)
    barrier = pltpu.get_barrier_semaphore()

    def body(d, _):
        pl.semaphore_signal(barrier, inc=1, device_id={axis: lax.rem(me + d, n)})
        return 0

    lax.fori_loop(1, n, body, 0)
    return barrier


def attention_kernel(
    n, tg, ow, mo, q, k, v, a, gq, gk, gv, ga, gow,
    pay, recv, gsend, grecv, upd_s, upd_p, ssem, rsem, gssem, grsem,
):
    me = lax.axis_index("sp")
    barrier = greet(n, "sp")
    tokens, lanes = q.shape
    blocks = tokens // BLOCK
    width = v.shape[1]
    heads = width // VAL_DIM
    rows = gow.shape[0]
    scale = KEY_CHANNELS ** (-0.5)

    cot = mm(tg[...], ow[...]).astype(BF16)
    row = lax.broadcasted_iota(jnp.int32, (tokens, tokens), 0)
    col = lax.broadcasted_iota(jnp.int32, (tokens, tokens), 1)
    same = (row // BLOCK) == (col // BLOCK)
    causal = same & (col <= row)
    cum = mm(jnp.where(causal, 1.0, 0.0), a[...], precision=HIGHEST)

    def spread(at):
        return jnp.concatenate(
            [
                jnp.broadcast_to(cum[b * BLOCK + at : b * BLOCK + at + 1], (BLOCK, lanes))
                for b in range(blocks)
            ],
            axis=0,
        )

    mid = spread(BLOCK // 2 - 1)
    end = spread(BLOCK - 1)
    qf = q[...].astype(F32) * scale
    kf = k[...].astype(F32)
    up_mid = jnp.exp(cum - mid)
    down_mid = jnp.exp(mid - cum)
    from_start = jnp.exp(cum)
    to_end = jnp.exp(end - cum)
    q_mid = (qf * up_mid).astype(BF16)
    k_mid = (kf * down_mid).astype(BF16)
    q_start = (qf * from_start).astype(BF16)
    k_end = (kf * to_end).astype(BF16)
    total = [cum[(b + 1) * BLOCK - 1 : (b + 1) * BLOCK] for b in range(blocks)]
    keep = [jnp.exp(t) for t in total]
    hrow = lax.broadcasted_iota(jnp.int32, (width, lanes), 0) // VAL_DIM
    hcol = lax.broadcasted_iota(jnp.int32, (width, lanes), 1) // KEY_CHANNELS
    headed = hrow == hcol

    def part(x, b):
        return x[b * BLOCK : (b + 1) * BLOCK]

    values = v[...]
    for b in range(blocks):
        upd_s[b] = jnp.where(headed, mm(part(values, b), part(k_end, b), 0, 0), 0.0)
        upd_p[b] = jnp.where(headed, mm(part(cot, b), part(q_start, b), 0, 0), 0.0)
    state = jnp.zeros((width, lanes), F32)
    pull = jnp.zeros((width, lanes), F32)
    for b in range(blocks):
        state = keep[b] * state + upd_s[b]
    for b in reversed(range(blocks)):
        pull = keep[b] * pull + upd_p[b]
    kept = jnp.exp(functools.reduce(lambda x, y: x + y, total))
    kept_hi = kept.astype(BF16)
    kept_lo = (kept - kept_hi.astype(F32)).astype(BF16)
    tail = jnp.concatenate(
        [jnp.broadcast_to(kept_hi.astype(F32), (8, lanes)), jnp.broadcast_to(kept_lo.astype(F32), (8, lanes))],
        axis=0,
    ).astype(BF16)

    def compact(x):
        return functools.reduce(
            lambda s, t: s + t, [x[h * VAL_DIM : (h + 1) * VAL_DIM] for h in range(heads)]
        )

    def expand(x):
        return jnp.where(headed, jnp.concatenate([x] * heads, axis=0), 0.0)

    pay[0, :VAL_DIM, :] = compact(state).astype(BF16)
    pay[1, :VAL_DIM, :] = compact(pull).astype(BF16)
    pay[0, VAL_DIM:, :] = tail
    pay[1, VAL_DIM:, :] = tail
    for j in range(tg.shape[1] // 256):
        gsend[j * 256 : (j + 1) * 256, :] = mm(
            tg[:, j * 256 : (j + 1) * 256], mo[...], 0, 0
        ).astype(BF16)
    pl.semaphore_wait(barrier, n - 1)

    def state_copy(d, slot):
        p = lax.rem(me + d, n)
        return pltpu.make_async_remote_copy(
            src_ref=pay.at[jnp.where(p > me, 0, 1)],
            dst_ref=recv.at[slot],
            send_sem=ssem.at[d],
            recv_sem=rsem.at[slot],
            device_id={"sp": p},
        )

    def grad_copy(d, slot):
        p = lax.rem(me + d, n)
        return pltpu.make_async_remote_copy(
            src_ref=gsend.at[pl.ds(pl.multiple_of(p * rows, rows), rows)],
            dst_ref=grecv.at[slot],
            send_sem=gssem.at[d],
            recv_sem=grsem.at[slot],
            device_id={"sp": p},
        )

    def each(f):
        def body(d, _):
            f(d)
            return 0

        lax.fori_loop(1, n, body, 0)

    each(lambda d: state_copy(d, me).start())
    each(lambda d: grad_copy(d, me).start())

    head_lane = lax.broadcasted_iota(jnp.int32, (tokens, lanes), 1) // KEY_CHANNELS
    dq = jnp.zeros((tokens, lanes), F32)
    dk = jnp.zeros((tokens, lanes), F32)
    dv = []
    for h in range(heads):
        cot_h = cot[:, h * VAL_DIM : (h + 1) * VAL_DIM]
        val_h = values[:, h * VAL_DIM : (h + 1) * VAL_DIM]
        q_h = jnp.where(head_lane == h, qf * up_mid, 0.0).astype(BF16)
        scores = jnp.where(causal, mm(q_h, k_mid, 1, 1), 0.0).astype(BF16)
        dscores = jnp.where(causal, mm(cot_h, val_h, 1, 1), 0.0).astype(BF16)
        dq = jnp.where(head_lane == h, mm(dscores, k_mid), dq)
        dk = jnp.where(head_lane == h, mm(dscores, q_mid, 0, 0), dk)
        dv.append(mm(scores, cot_h, 0, 0))
    dq = dq * up_mid
    dk = dk * down_mid
    dv = jnp.concatenate(dv, axis=1)

    each(lambda d: state_copy(d, lax.rem(me + d, n)).wait_recv())

    def follow(p, carry):
        ends = recv[p, VAL_DIM:, :].astype(F32)
        return (ends[0:1] + ends[8:9]) * carry + recv[p, :VAL_DIM, :].astype(F32)

    zero = jnp.zeros((VAL_DIM, lanes), F32)
    state = expand(lax.fori_loop(0, me, follow, zero))
    pull = expand(lax.fori_loop(0, n - 1 - me, lambda i, c: follow(n - 1 - i, c), zero))
    dq_in, after = [], []
    for b in range(blocks):
        dq_in.append(mm(part(cot, b), state.astype(BF16)))
        state = keep[b] * state + upd_s[b]
        after.append(state)
    dk_in, dv_in, edge = [None] * blocks, [None] * blocks, [None] * blocks
    for b in reversed(range(blocks)):
        low = pull.astype(BF16)
        dk_in[b] = mm(part(values, b), low)
        dv_in[b] = mm(part(k_end, b), low, 1, 1)
        edge[b] = jnp.broadcast_to(
            jnp.sum(after[b] * pull, axis=0, keepdims=True), (BLOCK, lanes)
        )
        pull = keep[b] * pull + upd_p[b]
    dq = dq + jnp.concatenate(dq_in, axis=0) * from_start
    dk = dk + jnp.concatenate(dk_in, axis=0) * to_end
    dv = dv + jnp.concatenate(dv_in, axis=0)
    gq[...] = (dq * scale).astype(BF16)
    gk[...] = dk.astype(BF16)
    gv[...] = dv.astype(BF16)
    flux = qf * dq - kf * dk
    later = jnp.where(same & (col >= row), 1.0, 0.0)
    ga[...] = mm(later, flux, precision=HIGHEST) + jnp.concatenate(edge, axis=0)

    each(lambda d: grad_copy(d, lax.rem(me + d, n)).wait_recv())
    own = gsend[pl.ds(pl.multiple_of(me * rows, rows), rows), :].astype(F32)
    gow[...] = lax.fori_loop(
        1, n, lambda d, t: t + grecv[lax.rem(me + d, n)].astype(F32), own
    )
    each(lambda d: state_copy(d, me).wait_send())
    each(lambda d: grad_copy(d, me).wait_send())


def attention_backward(token_grad, out_weight, mixer_out, query, key, value, log_decay):
    n = lax.axis_size("sp")
    tokens, lanes = query.shape
    width = value.shape[1]
    model = token_grad.shape[1]
    rows = model // n
    vm = pl.BlockSpec(memory_space=pltpu.VMEM)
    return pl.pallas_call(
        functools.partial(attention_kernel, n),
        out_shape=(
            jax.ShapeDtypeStruct((tokens, lanes), BF16),
            jax.ShapeDtypeStruct((tokens, lanes), BF16),
            jax.ShapeDtypeStruct((tokens, width), BF16),
            jax.ShapeDtypeStruct((tokens, lanes), F32),
            jax.ShapeDtypeStruct((rows, mixer_out.shape[1]), F32),
        ),
        in_specs=[vm] * 7,
        out_specs=(vm,) * 5,
        scratch_shapes=[
            pltpu.VMEM((2, VAL_DIM + 16, lanes), BF16),
            pltpu.VMEM((n, VAL_DIM + 16, lanes), BF16),
            pltpu.VMEM((model, mixer_out.shape[1]), BF16),
            pltpu.VMEM((n, rows, mixer_out.shape[1]), BF16),
            pltpu.VMEM((tokens // BLOCK, width, lanes), F32),
            pltpu.VMEM((tokens // BLOCK, width, lanes), F32),
            pltpu.SemaphoreType.DMA((n,)),
            pltpu.SemaphoreType.DMA((n,)),
            pltpu.SemaphoreType.DMA((n,)),
            pltpu.SemaphoreType.DMA((n,)),
        ],
        compiler_params=pltpu.CompilerParams(
            collective_id=0, has_side_effects=True, vmem_limit_bytes=24 * 1024 * 1024
        ),
        cost_estimate=pl.CostEstimate(
            flops=2 * 10**9, bytes_accessed=4 * 10**6, transcendentals=10**5
        ),
    )(token_grad, out_weight, mixer_out, query, key, value, log_decay)


def shards(
    moe_input,
    cotangent,
    expert_ids,
    route_weights,
    gate_weight,
    up_weight,
    down_weight,
    out_weight,
    mixer_out,
    query_vectors,
    key_vectors,
    value_vectors,
    log_decay,
):
    tok_count = moe_input.shape[0]
    model_width = moe_input.shape[1]
    slot_total = 2 * tok_count
    flat_ids = expert_ids.reshape(-1)
    sorting = jnp.argsort(flat_ids, stable=True)
    source_rows = sorting // 2
    inverse = jnp.argsort(sorting)
    gate_local = gate_weight[0]
    up_local = up_weight[0]
    down_local = down_weight[0]
    quarter = model_width // lax.axis_size("tp")
    offset = lax.axis_index("tp") * quarter
    own_input = lax.dynamic_slice_in_dim(moe_input, offset, quarter, 1)
    own_cot = lax.dynamic_slice_in_dim(cotangent, offset, quarter, 1)
    own_scaled = (route_weights[:, :, None] * own_cot[:, None, :].astype(jnp.float32)).astype(
        jnp.bfloat16
    )
    own_scaled = own_scaled.reshape(slot_total, quarter)
    arrived = (
        lax.all_to_all(own_input[source_rows], "sp", split_axis=0, concat_axis=0, tiled=True),
        lax.all_to_all(own_scaled[sorting], "sp", split_axis=0, concat_axis=0, tiled=True),
    )
    routed, routed_cot = (
        lax.all_gather(arrived[0], "tp", axis=1, tiled=True),
        lax.all_gather(arrived[1], "tp", axis=1, tiled=True),
    )
    grad_gate, grad_up, grad_down, partial_value = expert_pass(
        routed, routed_cot, gate_local, up_local, down_local
    )
    summed = lax.psum_scatter(
        partial_value.astype(jnp.bfloat16), "tp", scatter_dimension=1, tiled=True
    )
    returned = lax.all_to_all(summed, "sp", split_axis=0, concat_axis=0, tiled=True)
    per_slot = returned[inverse].reshape(tok_count, 2, quarter).astype(jnp.float32)
    own_grad = (own_cot.astype(jnp.float32) + per_slot[:, 0] + per_slot[:, 1]).astype(jnp.bfloat16)
    token_grad = lax.all_gather(own_grad, "tp", axis=1, tiled=True)
    gradients = attention_backward(
        token_grad, out_weight, mixer_out, query_vectors, key_vectors, value_vectors, log_decay
    )
    return (
        grad_gate[None],
        grad_up[None],
        grad_down[None],
        gradients[4],
        gradients[0],
        gradients[1],
        gradients[2],
        gradients[3],
    )


def solution(mesh):
    return jax.shard_map(
        shards,
        mesh=mesh,
        in_specs=(
            P("sp", None),
            P("sp", None),
            P("sp", None),
            P("sp", None),
            P("sp", None, "tp"),
            P("sp", None, "tp"),
            P("sp", "tp", None),
            P(None, "tp"),
            P("sp", "tp"),
            P("sp", "tp"),
            P("sp", "tp"),
            P("sp", "tp"),
            P("sp", "tp"),
        ),
        out_specs=(
            P("sp", None, "tp"),
            P("sp", None, "tp"),
            P("sp", "tp", None),
            P("sp", "tp"),
            P("sp", "tp"),
            P("sp", "tp"),
            P("sp", "tp"),
            P("sp", "tp"),
        ),
        check_vma=False,
    )
```

time: 287 us -> 204 us (0.71); the launches traced: 282 us -> 204 us
  blocking collectives: 112 us -> 36.2 us
  waiting for transfers between devices: 26.5 us -> 72.3 us
  other arithmetic: 53.2 us -> 10.6 us
  Pallas kernels: 0 us -> 34.2 us
  local copies, waits for them, and re-layouts: 32.3 us -> 14.3 us
  matrix products: 31.8 us -> 15.7 us
  starting transfers between devices: 10.8 us -> 6.16 us
    all_gather x3 -> x0, blocking collectives: 75.4 us -> none  [entering(): everything = jax.tree.map(lambda part: lax.all_gather(part, axis), shard)]
    pallas_call x0 -> x1, Pallas kernels: none -> 34.2 us  [attention_backward(): pl.pallas_call(functools.partial(attention_kernel, n), out_shape=(jax.Sha...]
    reduce_scatter x1, waiting for transfers between devices: 0.01 us -> 31.3 us  [shards(): lax.psum_scatter(partial_value.astype(jnp.bfloat16), 'tp', scatter_dimens...]
    reduce_sum x12 -> x0, other arithmetic: 17.2 us -> none  [the longest x4 16.3 us: block_step(): difference = cumulative[:, :, None, :] - cumulative[:, None, :, :]]
    while x8 -> x0, other arithmetic: 16 us -> none
    dot_general x32 -> x0, matrix products: 13.5 us -> none  [the longest x1 3.15 us: shards(): jnp.dot(token_grad.T, mixer_out, preferred_element_type=jnp.float32)]
    all_gather x1, waiting for transfers between devices: 2.27 us -> 10.6 us  [shards(): token_grad = lax.all_gather(own_grad, 'tp', axis=1, tiled=True)]
    another operation x20 -> x0, other arithmetic: 5.43 us -> none  [the longest x16 4.08 us: block_step(): cumulative = jnp.cumsum(decay_block, axis=1)]
  transfers between devices with their start and end apart: 6 -> 5, of which waited for: 4 -> 5; matrix products, arithmetic and copies ran while one was open for 32% -> 9% of each run, Pallas kernels for 0% -> 0%
where the time goes in v1:
time: 204 us
  waiting for transfers between devices  72.3 us (35%)
  blocking collectives  36.2 us (18%)
  Pallas kernels  34.2 us (17%)
  matrix products  15.7 us (8%)
  local copies, waits for them, and re-layouts  14.3 us (7%)
  between operations  14.1 us (7%)
  other arithmetic  10.6 us (5%)
  starting transfers between devices  6.16 us (3%)
    pallas_call x1, Pallas kernels, attention_backward(): pl.pallas_call(functools.partial(attention_kernel, n), out_shape=(jax.Sha...  34.2 us
    reduce_scatter x1, waiting for transfers between devices, shards(): lax.psum_scatter(partial_value.astype(jnp.bfloat16), 'tp', scatter_dimens...  31.3 us
    all_gather x1, waiting for transfers between devices, shards(): lax.all_gather(arrived[1], 'tp', axis=1, tiled=True)  20.9 us
    all_to_all x1, blocking collectives, shards(): lax.all_to_all(own_input[source_rows], 'sp', split_axis=0, concat_axis=0,...  18.5 us
    all_to_all x1, blocking collectives, shards(): lax.all_to_all(own_scaled[sorting], 'sp', split_axis=0, concat_axis=0, ti...  17.7 us
    all_gather x1, waiting for transfers between devices, shards(): token_grad = lax.all_gather(own_grad, 'tp', axis=1, tiled=True)  10.6 us
    all_to_all x1, waiting for transfers between devices, shards(): lax.all_to_all(summed, 'sp', split_axis=0, concat_axis=0, tiled=True)  7.27 us
    all_to_all x1, starting transfers between devices, shards(): lax.all_to_all(summed, 'sp', split_axis=0, concat_axis=0, tiled=True)  6.04 us
  transfers between devices with their start and end apart: 5, of which 5 were waited for; matrix products, arithmetic and copies ran while one was open for 9% of the time, Pallas kernels for 0%

profile of v1, /device:TPU:10, one launch (start us, length us, event | category | flops | bytes accessed | tf_op | source)
XLA Modules:
  0.0 203.6 jit_solution(455661635329496209)
XLA Ops:
  7.2 0.0 copy-start
  7.2 0.0 all-gather.4.cloned.1.call-start
  7.2 0.9 copy.21
  8.1 0.1 reshape.35
  8.3 3.8 %sort.34 = (s32[512]{0:T(512)}, s32[512]{0:T(512)S(1)}) sort(s32[512]{0:T(512)S(1)} %reshape.35, s32[512]{0:T(512)S(1)} %iota.8), dimensions={0}, to_apply=%region_0.0 | sort | flops 4608 | bytes 8192 | tf_op jit(solution)/shard_map/jit(argsort)/sort | solution.py:293
  12.1 1.1 dynamic-slice_convert_fusion
  13.2 2.0 gather_fusion
  15.2 18.5 %all_to_all.36 = bf16[8,64,512]{2,1,0:T(8,128)(2,1)} all-to-all(bf16[8,64,512]{2,1,0:T(8,128)(2,1)S(1)} %bitcast.50), channel_id=1, replica_groups=mesh['sp'=8,'tp'=4] {'sp'}, dimensions={0} | all-to-all | bytes 1048576 | tf_op jit(solution)/shard_map/all_to_all | solution.py:308
  33.6 0.0 all-gather.4.cloned.1.call-update
  33.6 0.0 all-gather.6.cloned.1.call-start
  33.7 0.4 mul.45
  34.1 0.7 mul.46
  34.8 0.0 copy-done.14
  34.8 0.1 copy.22
  34.9 0.1 mul.43
  35.1 0.1 multiply_convert_fusion
  35.2 2.0 gather_fusion.1
  37.2 17.7 %all_to_all.37 = bf16[8,64,512]{2,1,0:T(8,128)(2,1)} all-to-all(bf16[8,64,512]{2,1,0:T(8,128)(2,1)S(1)} %bitcast.51), channel_id=1, replica_groups=mesh['sp'=8,'tp'=4] {'sp'}, dimensions={0} | all-to-all | bytes 1048576 | tf_op jit(solution)/shard_map/all_to_all | solution.py:309
  54.9 0.0 all-gather.6.cloned.1.call-update
  55.0 0.0 reduce-scatter.2.cloned.1.call-start
  55.0 2.1 %all-gather.4.cloned.1.call-done = bf16[512,2048]{1,0:T(8,128)(2,1)} async-done(((bf16[512,512]{1,0:T(8,128)(2,1)}), bf16[512,2048]{1,0:T(8,128)(2,1)}) %all-gather.4.cloned.1.call-update) | async-done | bytes 2097168 | tf_op jit(solution)/shard_map/all_gather | solution.py:312
  57.1 0.0 copy-done
  57.1 2.4 %fusion.5 = f32[512,256]{1,0:T(8,128)S(1)} fusion(bf16[512,2048]{1,0:T(8,128)(2,1)} %all-gather.4.cloned.1.call-done, bf16[1,2048,256]{2,1,0:T(8,128)(2,1)S(1)} %copy-done), kind=kOutput, calls=%fused_computation.12 | convolution fusion | flops 536870912 | bytes 3670016 | tf_op jit(solution)/shard_map/dot_general | solution.py:24
  59.5 0.0 copy-done.9
  59.5 0.0 copy-done.15
  59.6 0.7 fusion.8
  60.3 0.0 copy-start.10
  60.3 20.9 %all-gather.6.cloned.1.call-done = bf16[512,2048]{1,0:T(8,128)(2,1)} async-done(((bf16[512,512]{1,0:T(8,128)(2,1)}), bf16[512,2048]{1,0:T(8,128)(2,1)}) %all-gather.6.cloned.1.call-update) | async-done | bytes 2097168 | tf_op jit(solution)/shard_map/all_gather | solution.py:313
  81.2 2.7 %multiply_convert_fusion.2 = (bf16[512,256]{1,0:T(8,128)(2,1)S(1)}, bf16[512,256]{1,0:T(8,128)(2,1)S(1)}) fusion(f32[512,256]{1,0:T(8,128)S(1)} %fusion.5, f32[512,256]{1,0:T(8,128)S(1)} %fusion.8, bf16[512,2048]{1,0:T(8,128)(2,1)} %all-gather.6.cloned.1.call-done, bf16[1,256,2048]{2,1,0:T(8,128)(2,1)} %param.19), kind=kOutput, calls=%fused_computation.26 | convolution fusion | flops 538574848 | bytes 4718592 | tf_op jit(solution)/shard_map/dot_general | solution.py:29
  83.9 0.0 copy-done.10
  83.9 0.0 copy-start.12
  83.9 0.7 fusion.3
  84.7 0.0 copy-done.12
  84.7 2.1 %add_convert_fusion = bf16[512,2048]{1,0:T(8,128)(2,1)} fusion(f32[512,2048]{1,0:T(8,128)S(1)} %fusion.3, bf16[512,256]{1,0:T(8,128)(2,1)S(1)} %get-tuple-element.24, bf16[1,2048,256]{2,1,0:T(8,128)(2,1)S(1)} %copy-done.9), kind=kOutput, calls=%fused_computation.3 | convolution fusion | flops 538968064 | bytes 7602176 | tf_op jit(solution)/shard_map/dot_general | solution.py:42
  86.8 0.0 reduce-scatter.2.cloned.1.call-update
  86.8 31.3 %reduce-scatter.2.cloned.1.call-done = bf16[512,512]{1,0:T(8,128)(2,1)} async-done(((bf16[512,2048]{1,0:T(8,128)(2,1)}), bf16[512,512]{1,0:T(8,128)(2,1)}) %reduce-scatter.2.cloned.1.call-update) | async-done | bytes 524304 | tf_op jit(solution)/shard_map/reduce_scatter | solution.py:318
  118.2 6.0 %all-to-all-start.2 = ((bf16[8,64,512]{2,1,0:T(8,128)(2,1)}), bf16[8,64,512]{2,1,0:T(8,128)(2,1)S(1)}, u32[]{:S(2)}, u32[]{:S(2)}) async-start(bf16[8,64,512]{2,1,0:T(8,128)(2,1)} %bitcast.54), calls=%async_computation.3 | async-start | bytes 1048576 | tf_op jit(solution)/shard_map/all_to_all | solution.py:321
  124.2 0.0 all-gather.8.cloned.1.call-start
  124.2 3.8 %sort.35 = (s32[512]{0:T(512)}, s32[512]{0:T(512)S(1)}) sort(s32[512]{0:T(512)S(1)} %get-tuple-element.15, s32[512]{0:T(512)S(1)} %iota.9), dimensions={0}, to_apply=%region_2.3 | sort | flops 4608 | bytes 8192 | tf_op jit(solution)/shard_map/jit(argsort)/sort | solution.py:295
  128.0 7.3 %all-to-all-done.2 = bf16[8,64,512]{2,1,0:T(8,128)(2,1)S(1)} async-done(((bf16[8,64,512]{2,1,0:T(8,128)(2,1)}), bf16[8,64,512]{2,1,0:T(8,128)(2,1)S(1)}, u32[]{:S(2)}, u32[]{:S(2)}) %all-to-all-start.2) | async-done | bytes 524320 | tf_op jit(solution)/shard_map/all_to_all | solution.py:321
  135.3 2.0 gather_fusion.2
  137.2 0.7 reshape.36
  137.9 0.8 fusion.20
  138.7 1.8 fusion.13
  140.5 0.0 all-gather.8.cloned.1.call-update
  140.6 0.0 copy-start.13
  140.6 0.0 copy-start.16
  140.6 3.5 %fusion = bf16[1,2048,256]{2,1,0:T(8,128)(2,1)} fusion(bf16[512,2048]{1,0:T(8,128)(2,1)} %all-gather.4.cloned.1.call-done, bf16[512,256]{1,0:T(8,128)(2,1)S(1)} %get-tuple-element.25), kind=kOutput, calls=%fused_computation.7 | convolution fusion | flops 537395200 | bytes 3407872 | tf_op jit(solution)/shard_map/dot_general | solution.py:37
  144.1 0.0 copy-done.13
  144.1 1.8 fusion.1
  145.8 0.0 copy-done.11
  145.8 0.0 copy-start.4
  145.9 0.0 copy-start.5
  145.9 0.0 copy-start.6
  145.9 0.0 copy-start.7
  145.9 1.8 fusion.2
  147.7 10.6 %all-gather.8.cloned.1.call-done.tg = bf16[256,2048]{1,0:T(8,128)(2,1)} async-done(((bf16[256,512]{1,0:T(8,128)(2,1)}), bf16[256,2048]{1,0:T(8,128)(2,1)}) %all-gather.8.cloned.1.call-update) | async-done | bytes 1048592 | tf_op jit(solution)/shard_map/all_gather | solution.py:324
  158.3 1.2 copy-done.2
  159.5 34.2 %shard_map.188 = (bf16[256,128]{1,0:T(8,128)(2,1)S(1)}, bf16[256,128]{1,0:T(8,128)(2,1)S(1)}, bf16[256,256]{1,0:T(8,128)(2,1)S(1)}, f32[256,128]{1,0:T(8,128)S(1)}, f32[256,256]{1,0:T(8,128)S(1)}) custom-call(bf16[256,2048]{1,0:T(8,128)(2,1)S(1)} %copy-done.2, bf16[2048,256]{1,0:T(8,128)(2,1)S(1)} %copy-done.1, bf16[256,256]{1,0:T(8,128)(2,1)S(1)} %copy-done.3, ...), custom_call_target="tpu_custom_call" | custom-call | flops 2000000000 | bytes 4000000 | tf_op jit(solution)/shard_map/pallas_call | solution.py:242
  193.8 0.7 copy.42
  194.5 0.6 copy.43
  195.1 0.6 copy.44
  195.8 0.7 copy.45
  196.4 0.7 copy.46
  (22 shorter events, 0.1 us)
Async XLA Ops:
  7.2 49.9 %copy-start = (bf16[1,2048,256]{2,1,0:T(8,128)(2,1)S(1)}, bf16[1,2048,256]{2,1,0:T(8,128)(2,1)}, u32[]{:S(2)}) copy-start(bf16[1,2048,256]{2,1,0:T(8,128)(2,1)} %param.17) | copy-start | bytes 3145732
  7.2 49.9 %all-gather.4.cloned.1.call-start = ((), (), s32[]{:S(2)}) async-start(), calls=%async_computation.4 | async-start | bytes 2621440 | tf_op jit(solution)/shard_map/all_gather | solution.py:312
  33.6 1.2 copy-start.14
  33.6 47.6 %all-gather.6.cloned.1.call-start = ((), (), s32[]{:S(2)}) async-start(), calls=%async_computation.5 | async-start | bytes 2621440 | tf_op jit(solution)/shard_map/all_gather | solution.py:313
  54.9 4.6 %copy-start.9 = (bf16[1,2048,256]{2,1,0:T(8,128)(2,1)S(1)}, bf16[1,2048,256]{2,1,0:T(8,128)(2,1)}, u32[]{:S(2)}) copy-start(bf16[1,2048,256]{2,1,0:T(8,128)(2,1)} %param.18) | copy-start | bytes 3145732
  55.0 63.2 %reduce-scatter.2.cloned.1.call-start = ((), (), s32[]{:S(2)}) async-start(), calls=%async_computation.6 | async-start | bytes 2621440 | tf_op jit(solution)/shard_map/reduce_scatter | solution.py:318
  57.1 2.5 %copy-start.15 = (bf16[512,2048]{1,0:T(8,128)(2,1)S(1)}, bf16[512,2048]{1,0:T(8,128)(2,1)}, u32[]{:S(2)}) copy-start(bf16[512,2048]{1,0:T(8,128)(2,1)} %all-gather.4.cloned.1.call-done) | copy-start | bytes 6291460
  60.3 23.6 %copy-start.10 = (f32[512,256]{1,0:T(8,128)}, f32[512,256]{1,0:T(8,128)S(1)}, u32[]{:S(2)}) copy-start(f32[512,256]{1,0:T(8,128)S(1)} %fusion.8) | copy-start | bytes 1572868
  83.9 0.8 copy-start.12
  118.2 17.1 %all-to-all-start.2 = ((bf16[8,64,512]{2,1,0:T(8,128)(2,1)}), bf16[8,64,512]{2,1,0:T(8,128)(2,1)S(1)}, u32[]{:S(2)}, u32[]{:S(2)}) async-start(bf16[8,64,512]{2,1,0:T(8,128)(2,1)} %bitcast.54), calls=%async_computation.3 | async-start | bytes 1048576 | tf_op jit(solution)/shard_map/all_to_all | solution.py:321
  124.2 34.1 %all-gather.8.cloned.1.call-start = ((), (), s32[]{:S(2)}) async-start(), calls=%async_computation.7 | async-start | bytes 1310720 | tf_op jit(solution)/shard_map/all_gather | solution.py:324
  140.6 3.5 %copy-start.13 = (bf16[512,256]{1,0:T(8,128)(2,1)S(1)}, bf16[512,256]{1,0:T(8,128)(2,1)}, u32[]{:S(2)}) copy-start(bf16[512,256]{1,0:T(8,128)(2,1)} %copy-done.12) | copy-start | bytes 786436
  140.6 3.5 %copy-start.16 = (bf16[512,2048]{1,0:T(8,128)(2,1)S(1)}, bf16[512,2048]{1,0:T(8,128)(2,1)}, u32[]{:S(2)}) copy-start(bf16[512,2048]{1,0:T(8,128)(2,1)} %all-gather.4.cloned.1.call-done) | copy-start | bytes 6291460
  144.1 1.8 copy-start.8
  144.1 1.8 copy-start.11
  145.8 12.5 %copy-start.1 = (bf16[2048,256]{1,0:T(8,128)(2,1)S(1)}, bf16[2048,256]{1,0:T(8,128)(2,1)}, u32[]{:S(2)}) copy-start(bf16[2048,256]{1,0:T(8,128)(2,1)} %ow.1) | copy-start | bytes 3145732
  145.8 12.5 %copy-start.3 = (bf16[256,256]{1,0:T(8,128)(2,1)S(1)}, bf16[256,256]{1,0:T(8,128)(2,1)}, u32[]{:S(2)}) copy-start(bf16[256,256]{1,0:T(8,128)(2,1)} %mo.1) | copy-start | bytes 393220
  145.8 12.4 %copy-start.4 = (bf16[256,256]{1,0:T(8,128)(2,1)S(1)}, bf16[256,256]{1,0:T(8,128)(2,1)}, u32[]{:S(2)}) copy-start(bf16[256,256]{1,0:T(8,128)(2,1)} %v.1) | copy-start | bytes 393220
  145.9 12.4 %copy-start.5 = (f32[256,128]{1,0:T(8,128)S(1)}, f32[256,128]{1,0:T(8,128)}, u32[]{:S(2)}) copy-start(f32[256,128]{1,0:T(8,128)} %a.1) | copy-start | bytes 393220
  145.9 12.4 %copy-start.6 = (bf16[256,128]{1,0:T(8,128)(2,1)S(1)}, bf16[256,128]{1,0:T(8,128)(2,1)}, u32[]{:S(2)}) copy-start(bf16[256,128]{1,0:T(8,128)(2,1)} %q.1) | copy-start | bytes 196612
  145.9 12.4 %copy-start.7 = (bf16[256,128]{1,0:T(8,128)(2,1)S(1)}, bf16[256,128]{1,0:T(8,128)(2,1)}, u32[]{:S(2)}) copy-start(bf16[256,128]{1,0:T(8,128)(2,1)} %k.1) | copy-start | bytes 196612
  158.3 1.2 copy-start.2
Sparse Core Ops, SparseCore 0:
  33.8 23.2 all-gather.3
  58.6 22.5 all-gather.5
  86.9 31.1 reduce-scatter.1
  140.7 17.5 all-gather.7

commit v2 on v1

--- a/solution.py
+++ b/solution.py
@@ -271,6 +271,268 @@
     )(token_grad, out_weight, mixer_out, query, key, value, log_decay)
 
 
+def placement(ids, slots, cap):
+    tokens = ids.shape[0]
+    lane = lax.broadcasted_iota(jnp.int32, (tokens, 128), 1)
+    first = ids[:, 0:1] == lane
+    second = ids[:, 1:2] == lane
+    named = jnp.where(first, 1.0, 0.0) + jnp.where(second, 1.0, 0.0)
+    row = lax.broadcasted_iota(jnp.int32, (tokens, tokens), 0)
+    col = lax.broadcasted_iota(jnp.int32, (tokens, tokens), 1)
+    before = mm(jnp.where(col < row, 1.0, 0.0).astype(BF16), named.astype(BF16))
+    at = before + (lane * cap).astype(F32)
+    slot = lax.broadcasted_iota(jnp.int32, (tokens, slots), 1).astype(F32)
+
+    def hot(mine):
+        place = jnp.sum(jnp.where(mine, at, 0.0), axis=1, keepdims=True)
+        return jnp.where(place == slot, 1.0, 0.0)
+
+    return hot(first), hot(second)
+
+
+def loop(start, stop, f):
+    def body(d, _):
+        f(d)
+        return 0
+
+    lax.fori_loop(start, stop, body, 0)
+
+
+def span(index, width):
+    return pl.ds(pl.multiple_of(index * width, width), width)
+
+
+def dispatch_kernel(n, x, cot, ids, weights, outx, outc, sx, sc, s1, r1, s2, r2):
+    me = lax.axis_index("sp")
+    place = lax.axis_index("tp")
+    half = lax.rem(place, 2)
+    sibling = place + 1 - 2 * half
+    barrier = greet(n, "sp")
+    pl.semaphore_signal(barrier, inc=1, device_id={"tp": sibling})
+    tokens, model = x.shape
+    width = model // 2
+    cap = outx.shape[1]
+    slots = n * cap
+    columns = span(half, width)
+    hot0, hot1 = placement(ids[...], slots, cap)
+    sent = mm((hot0 + hot1).astype(BF16), x[:, columns], 0, 0)
+    sx[...] = sent.reshape(n, cap, width).astype(BF16)
+    mine = cot[:, columns].astype(F32)
+    w = weights[...]
+    scaled = mm(hot0.astype(BF16), (w[:, 0:1] * mine).astype(BF16), 0, 0)
+    scaled = scaled + mm(hot1.astype(BF16), (w[:, 1:2] * mine).astype(BF16), 0, 0)
+    sc[...] = scaled.reshape(n, cap, width).astype(BF16)
+    outx[me, :, columns] = sx[me]
+    outc[me, :, columns] = sc[me]
+    pl.semaphore_wait(barrier, n)
+    pairs = ((0, sx, outx), (1, sc, outc))
+
+    def first(i, source, out, d, slot):
+        p = lax.rem(me + d, n)
+        return pltpu.make_async_remote_copy(
+            src_ref=source.at[p],
+            dst_ref=out.at[slot, :, columns],
+            send_sem=s1.at[i, d],
+            recv_sem=r1.at[i, slot],
+            device_id={"sp": p},
+        )
+
+    def second(i, src, out, slot, cols):
+        return pltpu.make_async_remote_copy(
+            src_ref=src,
+            dst_ref=out.at[slot, :, cols],
+            send_sem=s2.at[i, slot],
+            recv_sem=r2.at[i, slot],
+            device_id={"tp": sibling},
+        )
+
+    for i, source, out in pairs:
+        loop(1, n, lambda d: first(i, source, out, d, me).start())
+    for i, source, out in pairs:
+        second(i, source.at[me], out, me, columns).start()
+    for i, source, out in pairs:
+
+        def forward(d):
+            slot = lax.rem(me - d + n, n)
+            first(i, source, out, d, slot).wait_recv()
+            second(i, out.at[slot, :, columns], out, slot, columns).start()
+
+        loop(1, n, forward)
+    theirs = span(1 - half, width)
+    for i, source, out in pairs:
+        loop(0, n, lambda s: second(i, source.at[s], out, s, theirs).wait_recv())
+        loop(1, n, lambda d: first(i, source, out, d, me).wait_send())
+        loop(0, n, lambda s: second(i, source.at[s], out, s, columns).wait_send())
+
+
+def dispatch(x, cot, ids, weights):
+    n = lax.axis_size("sp")
+    tokens, model = x.shape
+    cap = 2 * tokens // n
+    vm = pl.BlockSpec(memory_space=pltpu.VMEM)
+    shape = jax.ShapeDtypeStruct((n, cap, model), BF16)
+    buffer = pltpu.VMEM((n, cap, model // 2), BF16)
+    sems = pltpu.SemaphoreType.DMA((2, n))
+    outs = pl.pallas_call(
+        functools.partial(dispatch_kernel, n),
+        out_shape=(shape, shape),
+        in_specs=[vm] * 4,
+        out_specs=(vm, vm),
+        scratch_shapes=[buffer, buffer, sems, sems, sems, sems],
+        compiler_params=pltpu.CompilerParams(
+            collective_id=1, has_side_effects=True, vmem_limit_bytes=32 * 1024 * 1024
+        ),
+    )(x, cot, ids, weights)
+    return [out.reshape(n * cap, model) for out in outs]
+
+
+def return_kernel(
+    n, part, cot, ids, tg, got, to_far, far, to_home, home, quarter,
+    s1, r1, s2, r2, s3, r3, s4, r4,
+):
+    me = lax.axis_index("sp")
+    place = lax.axis_index("tp")
+    core = lax.rem(place, 2)
+    side = lax.div(place, 2)
+    sibling = place + 1 - 2 * core
+    opposite = lax.rem(place + 2, 4)
+    barrier = greet(n, "sp")
+    pl.semaphore_signal(barrier, inc=1, device_id={"tp": sibling})
+    pl.semaphore_signal(barrier, inc=1, device_id={"tp": opposite})
+    tokens, model = cot.shape
+    cap = part.shape[1]
+    slots = n * cap
+    wide, slim = model // 2, model // 4
+    mine = span(2 * core + side, slim)
+    other = span(2 * core + 1 - side, slim)
+    pl.semaphore_wait(barrier, n + 1)
+
+    def near(p):
+        return pltpu.make_async_remote_copy(
+            src_ref=part.at[p, :, span(1 - core, wide)],
+            dst_ref=got.at[p],
+            send_sem=s1.at[p],
+            recv_sem=r1.at[p],
+            device_id={"tp": sibling},
+        )
+
+    def across(p):
+        return pltpu.make_async_remote_copy(
+            src_ref=to_far.at[p],
+            dst_ref=far.at[p],
+            send_sem=s2.at[p],
+            recv_sem=r2.at[p],
+            device_id={"tp": opposite},
+        )
+
+    def back(d, slot):
+        p = lax.rem(me + d, n)
+        return pltpu.make_async_remote_copy(
+            src_ref=to_home.at[p],
+            dst_ref=home.at[slot],
+            send_sem=s3.at[d],
+            recv_sem=r3.at[slot],
+            device_id={"sp": p},
+        )
+
+    def to(d):
+        return lax.rem(me + d, n)
+
+    loop(1, n + 1, lambda d: near(to(d)).start())
+    hot0, hot1 = placement(ids[...], slots, cap)
+
+    def stage_far(d):
+        p = to(d)
+        near(p).wait_recv()
+        to_far[p] = (
+            part[p, :, other].astype(F32) + got[p, :, span(1 - side, slim)].astype(F32)
+        ).astype(BF16)
+
+        @pl.when(d > 1)
+        def _():
+            across(to(d - 1)).start()
+
+    loop(1, n + 1, stage_far)
+    across(me).start()
+
+    def stage_home(d):
+        p = to(d)
+        across(p).wait_recv()
+        to_home[p] = (
+            part[p, :, mine].astype(F32)
+            + got[p, :, span(side, slim)].astype(F32)
+            + far[p].astype(F32)
+        ).astype(BF16)
+
+        @pl.when(d > 1)
+        def _():
+            back(d - 1, me).start()
+
+    loop(1, n + 1, stage_home)
+    home[me] = to_home[me]
+    loop(1, n, lambda d: back(d, to(d)).wait_recv())
+    rows = home[...].astype(F32).reshape(slots, slim).astype(BF16)
+    total = cot[:, mine].astype(F32) + mm(hot0.astype(BF16), rows)
+    total = (total + mm(hot1.astype(BF16), rows)).astype(BF16)
+    quarter[...] = total
+    tg[:, mine] = total
+    pieces = 4
+    size = tokens // pieces
+
+    def share(i, kind, src, cols, target):
+        return pltpu.make_async_remote_copy(
+            src_ref=src,
+            dst_ref=tg.at[span(i, size), cols],
+            send_sem=s4.at[kind, i],
+            recv_sem=r4.at[kind, i],
+            device_id={"tp": target},
+        )
+
+    def own(i):
+        return quarter.at[span(i, size)]
+
+    theirs = span(2 * (1 - core) + side, slim)
+    theirs_far = span(2 * (1 - core) + 1 - side, slim)
+    loop(0, pieces, lambda i: share(i, 0, own(i), mine, opposite).start())
+    loop(0, pieces, lambda i: share(i, 1, own(i), mine, sibling).start())
+
+    def relay(i):
+        share(i, 0, own(i), other, opposite).wait_recv()
+        share(i, 2, tg.at[span(i, size), other], other, sibling).start()
+
+    loop(0, pieces, relay)
+    loop(0, pieces, lambda i: share(i, 1, own(i), theirs, sibling).wait_recv())
+    loop(0, pieces, lambda i: share(i, 2, own(i), theirs_far, sibling).wait_recv())
+    loop(0, n, lambda p: near(p).wait_send())
+    loop(0, n, lambda p: across(p).wait_send())
+    loop(1, n, lambda d: back(d, me).wait_send())
+    for kind, target in ((0, opposite), (1, sibling), (2, sibling)):
+        loop(0, pieces, lambda i: share(i, kind, own(i), mine, target).wait_send())
+
+
+def give_back(partial_value, cot, ids):
+    n = lax.axis_size("sp")
+    tokens, model = cot.shape
+    cap = 2 * tokens // n
+    vm = pl.BlockSpec(memory_space=pltpu.VMEM)
+    slim = pltpu.VMEM((n, cap, model // 4), BF16)
+    sems = pltpu.SemaphoreType.DMA((n,))
+    shared = pltpu.SemaphoreType.DMA((3, 4))
+    return pl.pallas_call(
+        functools.partial(return_kernel, n),
+        out_shape=jax.ShapeDtypeStruct((tokens, model), BF16),
+        in_specs=[vm] * 3,
+        out_specs=vm,
+        scratch_shapes=[pltpu.VMEM((n, cap, model // 2), BF16), slim, slim, slim, slim]
+        + [pltpu.VMEM((tokens, model // 4), BF16)]
+        + [sems] * 6
+        + [shared] * 2,
+        compiler_params=pltpu.CompilerParams(
+            collective_id=2, has_side_effects=True, vmem_limit_bytes=32 * 1024 * 1024
+        ),
+    )(partial_value.reshape(n, cap, model), cot, ids)
+
+
 def shards(
     moe_input,
     cotangent,
@@ -286,42 +548,11 @@
     value_vectors,
     log_decay,
 ):
-    tok_count = moe_input.shape[0]
-    model_width = moe_input.shape[1]
-    slot_total = 2 * tok_count
-    flat_ids = expert_ids.reshape(-1)
-    sorting = jnp.argsort(flat_ids, stable=True)
-    source_rows = sorting // 2
-    inverse = jnp.argsort(sorting)
-    gate_local = gate_weight[0]
-    up_local = up_weight[0]
-    down_local = down_weight[0]
-    quarter = model_width // lax.axis_size("tp")
-    offset = lax.axis_index("tp") * quarter
-    own_input = lax.dynamic_slice_in_dim(moe_input, offset, quarter, 1)
-    own_cot = lax.dynamic_slice_in_dim(cotangent, offset, quarter, 1)
-    own_scaled = (route_weights[:, :, None] * own_cot[:, None, :].astype(jnp.float32)).astype(
-        jnp.bfloat16
-    )
-    own_scaled = own_scaled.reshape(slot_total, quarter)
-    arrived = (
-        lax.all_to_all(own_input[source_rows], "sp", split_axis=0, concat_axis=0, tiled=True),
-        lax.all_to_all(own_scaled[sorting], "sp", split_axis=0, concat_axis=0, tiled=True),
-    )
-    routed, routed_cot = (
-        lax.all_gather(arrived[0], "tp", axis=1, tiled=True),
-        lax.all_gather(arrived[1], "tp", axis=1, tiled=True),
-    )
+    routed, routed_cot = dispatch(moe_input, cotangent, expert_ids, route_weights)
     grad_gate, grad_up, grad_down, partial_value = expert_pass(
-        routed, routed_cot, gate_local, up_local, down_local
-    )
-    summed = lax.psum_scatter(
-        partial_value.astype(jnp.bfloat16), "tp", scatter_dimension=1, tiled=True
-    )
-    returned = lax.all_to_all(summed, "sp", split_axis=0, concat_axis=0, tiled=True)
-    per_slot = returned[inverse].reshape(tok_count, 2, quarter).astype(jnp.float32)
-    own_grad = (own_cot.astype(jnp.float32) + per_slot[:, 0] + per_slot[:, 1]).astype(jnp.bfloat16)
-    token_grad = lax.all_gather(own_grad, "tp", axis=1, tiled=True)
+        routed, routed_cot, gate_weight[0], up_weight[0], down_weight[0]
+    )
+    token_grad = give_back(partial_value.astype(jnp.bfloat16), cotangent, expert_ids)
     gradients = attention_backward(
         token_grad, out_weight, mixer_out, query_vectors, key_vectors, value_vectors, log_decay
     )

time: 204 us -> 138 us (0.68)
  Pallas kernels: 34.2 us -> 119 us
  waiting for transfers between devices: 72.3 us -> 0 us
  blocking collectives: 36.2 us -> 0 us
  between operations: 14.1 us -> 0.82 us
  other arithmetic: 10.6 us -> 0 us
  matrix products: 15.7 us -> 9.02 us
  starting transfers between devices: 6.16 us -> 0 us
  local copies, waits for them, and re-layouts: 14.3 us -> 8.92 us
    pallas_call x0 -> x2, Pallas kernels: none -> 84.9 us  [the longest x1 51 us: dispatch(): pl.pallas_call(functools.partial(dispatch_kernel, n), out_shape=(shape, s...]
    all_to_all x2 -> x0, blocking collectives: 36.2 us -> none  [the longest x1 18.5 us: shards(): lax.all_to_all(own_input[source_rows], 'sp', split_axis=0, concat_axis=0,...]
    all_gather x3 -> x0, waiting for transfers between devices: 33.6 us -> none  [the longest x1 20.9 us: shards(): lax.all_gather(arrived[1], 'tp', axis=1, tiled=True)]
    reduce_scatter x1 -> x0, waiting for transfers between devices: 31.3 us -> none  [shards(): lax.psum_scatter(partial_value.astype(jnp.bfloat16), 'tp', scatter_dimens...]
    sort x2 -> x0, other arithmetic: 7.54 us -> none  [the longest x1 3.77 us: shards(): sorting = jnp.argsort(flat_ids, stable=True)]
    all_to_all x1 -> x0, waiting for transfers between devices: 7.27 us -> none  [shards(): lax.all_to_all(summed, 'sp', split_axis=0, concat_axis=0, tiled=True)]
    all_to_all x1 -> x0, starting transfers between devices: 6.04 us -> none  [shards(): lax.all_to_all(summed, 'sp', split_axis=0, concat_axis=0, tiled=True)]
    gather x3 -> x0, local copies, waits for them, and re-layouts: 5.91 us -> none  [the longest x1 1.97 us: shards(): own_input[source_rows]]
  transfers between devices with their start and end apart: 5 -> 0, of which waited for: 5 -> 0; matrix products, arithmetic and copies ran while one was open for 9% -> 0% of each run, Pallas kernels for 0% -> 0%
where the time goes in v2:
time: 138 us
  Pallas kernels  119 us (86%)
  matrix products  9.02 us (7%)
  local copies, waits for them, and re-layouts  8.92 us (6%)
    pallas_call x1, Pallas kernels, dispatch(): pl.pallas_call(functools.partial(dispatch_kernel, n), out_shape=(shape, s...  51 us
    pallas_call x1, Pallas kernels, attention_backward(): pl.pallas_call(functools.partial(attention_kernel, n), out_shape=(jax.Sha...  34 us
    pallas_call x1, Pallas kernels, give_back(): pl.pallas_call(functools.partial(return_kernel, n), out_shape=jax.ShapeDt...  33.9 us
    unnamed x31, local copies, waits for them, and re-layouts  8.92 us

profile of v2, /device:TPU:10, one launch (start us, length us, event | category | flops | bytes accessed | tf_op | source)
XLA Modules:
  0.0 137.7 jit_solution(12054597954654409755)
XLA Ops:
  0.6 0.0 copy-start
  0.6 0.9 copy.21.ids
  1.6 0.8 copy.22.weights
  2.4 0.0 copy-start.1
  2.4 1.2 copy-done.1
  3.6 0.0 copy-start.3
  3.6 1.2 copy-done.3
  4.8 51.0 %shard_map.188 = (bf16[8,64,2048]{2,1,0:T(8,128)(2,1)S(1)}, bf16[8,64,2048]{2,1,0:T(8,128)(2,1)S(1)}) custom-call(bf16[256,2048]{1,0:T(8,128)(2,1)S(1)} %copy-done.3, bf16[256,2048]{1,0:T(8,128)(2,1)S(1)} %copy-done.1, s32[256,2]{1,0:T(8,128)S(1)} %copy.21.ids, f32[256,2]{1,0:T(8,128)S(1)} %copy.22.weights), custom_call_target="tpu_custom_call" | custom-call | tf_op jit(solution)/shard_map/pallas_call | solution.py:376
  55.9 0.0 copy-start.10
  55.9 0.0 copy-done
  55.9 0.7 fusion.5
  56.6 0.5 copy-done.10
  57.1 0.0 copy-start.11
  57.1 0.7 fusion.8
  57.8 0.5 copy-done.11
  58.3 0.8 multiply_convert_fusion.1
  59.2 1.8 %fusion.2 = bf16[1,256,2048]{2,1,0:T(8,128)(2,1)} fusion(bf16[512,2048]{1,0:T(8,128)(2,1)S(1)} %bitcast.36, f32[512,256]{1,0:T(8,128)S(1)} %fusion.8, f32[512,256]{1,0:T(8,128)S(1)} %fusion.5), kind=kOutput, calls=%fused_computation.6 | convolution fusion | flops 538181632 | bytes 4194304 | tf_op jit(solution)/shard_map/dot_general | solution.py:30
  61.0 1.8 %fusion.1 = bf16[1,2048,256]{2,1,0:T(8,128)(2,1)} fusion(bf16[512,2048]{1,0:T(8,128)(2,1)S(1)} %bitcast.39, bf16[512,256]{1,0:T(8,128)(2,1)S(1)} %get-tuple-element.22), kind=kOutput, calls=%fused_computation.5 | convolution fusion | flops 537395200 | bytes 3407872 | tf_op jit(solution)/shard_map/dot_general | solution.py:40
  62.7 1.7 %fusion = bf16[1,2048,256]{2,1,0:T(8,128)(2,1)} fusion(bf16[512,2048]{1,0:T(8,128)(2,1)S(1)} %bitcast.40, bf16[512,256]{1,0:T(8,128)(2,1)S(1)} %get-tuple-element.23), kind=kOutput, calls=%fused_computation.4 | convolution fusion | flops 537395200 | bytes 3407872 | tf_op jit(solution)/shard_map/dot_general | solution.py:37
  64.5 0.7 fusion.3
  65.2 0.0 copy-start.2
  65.2 0.7 add_convert_fusion
  66.0 0.5 copy-done.2
  66.4 0.0 copy-start.4
  66.4 0.0 copy-start.5
  66.4 0.0 copy-start.6
  66.4 0.0 copy-start.7
  66.4 0.0 copy-start.8
  66.4 0.0 copy-start.9
  66.5 33.9 %shard_map.189.tg = bf16[256,2048]{1,0:T(8,128)(2,1)S(1)} custom-call(bf16[8,64,2048]{2,1,0:T(8,128)(2,1)S(1)} %bitcast.34, bf16[256,2048]{1,0:T(8,128)(2,1)S(1)} %copy-done.2, s32[256,2]{1,0:T(8,128)S(1)} %copy.21.ids), custom_call_target="tpu_custom_call" | custom-call | tf_op jit(solution)/shard_map/pallas_call | solution.py:521
  100.3 0.0 copy-done.4
  100.3 0.0 copy-done.5
  100.3 0.0 copy-done.6
  100.4 0.0 copy-done.7
  100.4 0.0 copy-done.8
  100.4 0.0 copy-done.9
  100.4 34.0 %shard_map.190 = (bf16[256,128]{1,0:T(8,128)(2,1)S(1)}, bf16[256,128]{1,0:T(8,128)(2,1)S(1)}, bf16[256,256]{1,0:T(8,128)(2,1)S(1)}, f32[256,128]{1,0:T(8,128)S(1)}, f32[256,256]{1,0:T(8,128)S(1)}) custom-call(bf16[256,2048]{1,0:T(8,128)(2,1)S(1)} %shard_map.189.tg, bf16[2048,256]{1,0:T(8,128)(2,1)S(1)} %copy-done.4, bf16[256,256]{1,0:T(8,128)(2,1)S(1)} %copy-done.5, ...), custom_call_target="tpu_custom_call" | custom-call | flops 2000000000 | bytes 4000000 | tf_op jit(solution)/shard_map/pallas_call | solution.py:242
  134.4 0.7 copy.29
  135.1 0.6 copy.30
  135.8 0.6 copy.31
  136.4 0.7 copy.32
  137.0 0.7 copy.33
Async XLA Ops:
  0.6 55.3 %copy-start = (bf16[1,2048,256]{2,1,0:T(8,128)(2,1)S(1)}, bf16[1,2048,256]{2,1,0:T(8,128)(2,1)}, u32[]{:S(2)}) copy-start(bf16[1,2048,256]{2,1,0:T(8,128)(2,1)} %param.17) | copy-start | bytes 3145732
  2.4 1.2 copy-start.1
  3.6 1.2 copy-start.3
  55.9 1.2 copy-start.10
  57.1 1.2 copy-start.11
  65.2 1.2 copy-start.2
  66.4 33.9 %copy-start.4 = (bf16[2048,256]{1,0:T(8,128)(2,1)S(1)}, bf16[2048,256]{1,0:T(8,128)(2,1)}, u32[]{:S(2)}) copy-start(bf16[2048,256]{1,0:T(8,128)(2,1)} %ow.1) | copy-start | bytes 3145732
  66.4 33.9 %copy-start.5 = (bf16[256,256]{1,0:T(8,128)(2,1)S(1)}, bf16[256,256]{1,0:T(8,128)(2,1)}, u32[]{:S(2)}) copy-start(bf16[256,256]{1,0:T(8,128)(2,1)} %mo.1) | copy-start | bytes 393220
  66.4 33.9 %copy-start.6 = (bf16[256,256]{1,0:T(8,128)(2,1)S(1)}, bf16[256,256]{1,0:T(8,128)(2,1)}, u32[]{:S(2)}) copy-start(bf16[256,256]{1,0:T(8,128)(2,1)} %v.1) | copy-start | bytes 393220
  66.4 33.9 %copy-start.7 = (f32[256,128]{1,0:T(8,128)S(1)}, f32[256,128]{1,0:T(8,128)}, u32[]{:S(2)}) copy-start(f32[256,128]{1,0:T(8,128)} %a.1) | copy-start | bytes 393220
  66.4 33.9 %copy-start.8 = (bf16[256,128]{1,0:T(8,128)(2,1)S(1)}, bf16[256,128]{1,0:T(8,128)(2,1)}, u32[]{:S(2)}) copy-start(bf16[256,128]{1,0:T(8,128)(2,1)} %q.1) | copy-start | bytes 196612
  66.4 33.9 %copy-start.9 = (bf16[256,128]{1,0:T(8,128)(2,1)S(1)}, bf16[256,128]{1,0:T(8,128)(2,1)}, u32[]{:S(2)}) copy-start(bf16[256,128]{1,0:T(8,128)(2,1)} %k.1) | copy-start | bytes 196612

commit v3 on v2

--- a/solution.py
+++ b/solution.py
@@ -305,15 +305,19 @@
 def dispatch_kernel(n, x, cot, ids, weights, outx, outc, sx, sc, s1, r1, s2, r2):
     me = lax.axis_index("sp")
     place = lax.axis_index("tp")
-    half = lax.rem(place, 2)
-    sibling = place + 1 - 2 * half
+    core = lax.rem(place, 2)
+    side = lax.div(place, 2)
+    sibling = place + 1 - 2 * core
+    opposite = lax.rem(place + 2, 4)
     barrier = greet(n, "sp")
     pl.semaphore_signal(barrier, inc=1, device_id={"tp": sibling})
+    pl.semaphore_signal(barrier, inc=1, device_id={"tp": opposite})
     tokens, model = x.shape
-    width = model // 2
+    width = model // 4
     cap = outx.shape[1]
     slots = n * cap
-    columns = span(half, width)
+    columns = span(2 * core + side, width)
+    other = span(2 * core + 1 - side, width)
     hot0, hot1 = placement(ids[...], slots, cap)
     sent = mm((hot0 + hot1).astype(BF16), x[:, columns], 0, 0)
     sx[...] = sent.reshape(n, cap, width).astype(BF16)
@@ -324,7 +328,7 @@
     sc[...] = scaled.reshape(n, cap, width).astype(BF16)
     outx[me, :, columns] = sx[me]
     outc[me, :, columns] = sc[me]
-    pl.semaphore_wait(barrier, n)
+    pl.semaphore_wait(barrier, n + 1)
     pairs = ((0, sx, outx), (1, sc, outc))
 
     def first(i, source, out, d, slot):
@@ -337,32 +341,45 @@
             device_id={"sp": p},
         )
 
-    def second(i, src, out, slot, cols):
+    def second(i, kind, src, out, slot, cols):
         return pltpu.make_async_remote_copy(
             src_ref=src,
             dst_ref=out.at[slot, :, cols],
-            send_sem=s2.at[i, slot],
-            recv_sem=r2.at[i, slot],
-            device_id={"tp": sibling},
-        )
+            send_sem=s2.at[2 * kind + i, slot],
+            recv_sem=r2.at[2 * kind + i, slot],
+            device_id={"tp": opposite if kind == 0 else sibling},
+        )
+
+    def relay(i, out, d):
+        slot = lax.rem(me - d + n, n)
+        second(i, 0, out.at[slot, :, other], out, slot, other).wait_recv()
+        second(i, 2, out.at[slot, :, other], out, slot, other).start()
 
     for i, source, out in pairs:
         loop(1, n, lambda d: first(i, source, out, d, me).start())
     for i, source, out in pairs:
-        second(i, source.at[me], out, me, columns).start()
+        for kind in (0, 1):
+            second(i, kind, source.at[me], out, me, columns).start()
     for i, source, out in pairs:
 
         def forward(d):
             slot = lax.rem(me - d + n, n)
             first(i, source, out, d, slot).wait_recv()
-            second(i, out.at[slot, :, columns], out, slot, columns).start()
+            for kind in (0, 1):
+                second(i, kind, out.at[slot, :, columns], out, slot, columns).start()
+            relay(i, out, d - 1)
 
         loop(1, n, forward)
-    theirs = span(1 - half, width)
     for i, source, out in pairs:
-        loop(0, n, lambda s: second(i, source.at[s], out, s, theirs).wait_recv())
+        relay(i, out, n - 1)
+    theirs = span(2 * (1 - core) + side, width)
+    theirs_far = span(2 * (1 - core) + 1 - side, width)
+    for i, source, out in pairs:
+        loop(0, n, lambda s: second(i, 1, source.at[s], out, s, theirs).wait_recv())
+        loop(0, n, lambda s: second(i, 2, source.at[s], out, s, theirs_far).wait_recv())
         loop(1, n, lambda d: first(i, source, out, d, me).wait_send())
-        loop(0, n, lambda s: second(i, source.at[s], out, s, columns).wait_send())
+        for kind in (0, 1, 2):
+            loop(0, n, lambda s: second(i, kind, source.at[s], out, s, columns).wait_send())
 
 
 def dispatch(x, cot, ids, weights):
@@ -371,14 +388,15 @@
     cap = 2 * tokens // n
     vm = pl.BlockSpec(memory_space=pltpu.VMEM)
     shape = jax.ShapeDtypeStruct((n, cap, model), BF16)
-    buffer = pltpu.VMEM((n, cap, model // 2), BF16)
+    buffer = pltpu.VMEM((n, cap, model // 4), BF16)
     sems = pltpu.SemaphoreType.DMA((2, n))
+    more = pltpu.SemaphoreType.DMA((6, n))
     outs = pl.pallas_call(
         functools.partial(dispatch_kernel, n),
         out_shape=(shape, shape),
         in_specs=[vm] * 4,
         out_specs=(vm, vm),
-        scratch_shapes=[buffer, buffer, sems, sems, sems, sems],
+        scratch_shapes=[buffer, buffer, sems, sems, more, more],
         compiler_params=pltpu.CompilerParams(
             collective_id=1, has_side_effects=True, vmem_limit_bytes=32 * 1024 * 1024
         ),

time: 138 us -> 131 us (0.949)
  Pallas kernels: 119 us -> 112 us
    pallas_call x1, Pallas kernels: 51 us -> 41.4 us  [dispatch(): pl.pallas_call(functools.partial(dispatch_kernel, n), out_shape=(shape, s...]
    pallas_call x1, Pallas kernels: 33.9 us -> 36.8 us  [give_back(): pl.pallas_call(functools.partial(return_kernel, n), out_shape=jax.ShapeDt...]
where the time goes in v3:
time: 131 us
  Pallas kernels  112 us (85%)
  matrix products  9.02 us (7%)
  local copies, waits for them, and re-layouts  8.92 us (7%)
    pallas_call x1, Pallas kernels, dispatch(): pl.pallas_call(functools.partial(dispatch_kernel, n), out_shape=(shape, s...  41.4 us
    pallas_call x1, Pallas kernels, give_back(): pl.pallas_call(functools.partial(return_kernel, n), out_shape=jax.ShapeDt...  36.8 us
    pallas_call x1, Pallas kernels, attention_backward(): pl.pallas_call(functools.partial(attention_kernel, n), out_shape=(jax.Sha...  33.7 us
    unnamed x31, local copies, waits for them, and re-layouts  8.92 us

profile of v3, /device:TPU:10, one launch (start us, length us, event | category | flops | bytes accessed | tf_op | source)
XLA Modules:
  0.0 130.6 jit_solution(534609774135462447)
XLA Ops:
  0.6 0.0 copy-start
  0.6 0.9 copy.21.ids
  1.6 0.8 copy.22.weights
  2.4 0.0 copy-start.1
  2.4 1.2 copy-done.1
  3.6 0.0 copy-start.3
  3.6 1.2 copy-done.3
  4.8 41.4 %shard_map.188 = (bf16[8,64,2048]{2,1,0:T(8,128)(2,1)S(1)}, bf16[8,64,2048]{2,1,0:T(8,128)(2,1)S(1)}) custom-call(bf16[256,2048]{1,0:T(8,128)(2,1)S(1)} %copy-done.3, bf16[256,2048]{1,0:T(8,128)(2,1)S(1)} %copy-done.1, s32[256,2]{1,0:T(8,128)S(1)} %copy.21.ids, f32[256,2]{1,0:T(8,128)S(1)} %copy.22.weights), custom_call_target="tpu_custom_call" | custom-call | tf_op jit(solution)/shard_map/pallas_call | solution.py:394
  46.2 0.0 copy-start.10
  46.2 0.0 copy-done
  46.2 0.7 fusion.5
  47.0 0.5 copy-done.10
  47.4 0.0 copy-start.11
  47.5 0.7 fusion.8
  48.2 0.5 copy-done.11
  48.7 0.8 multiply_convert_fusion.1
  49.5 1.8 %fusion.2 = bf16[1,256,2048]{2,1,0:T(8,128)(2,1)} fusion(bf16[512,2048]{1,0:T(8,128)(2,1)S(1)} %bitcast.36, f32[512,256]{1,0:T(8,128)S(1)} %fusion.8, f32[512,256]{1,0:T(8,128)S(1)} %fusion.5), kind=kOutput, calls=%fused_computation.6 | convolution fusion | flops 538181632 | bytes 4194304 | tf_op jit(solution)/shard_map/dot_general | solution.py:30
  51.3 1.8 %fusion.1 = bf16[1,2048,256]{2,1,0:T(8,128)(2,1)} fusion(bf16[512,2048]{1,0:T(8,128)(2,1)S(1)} %bitcast.39, bf16[512,256]{1,0:T(8,128)(2,1)S(1)} %get-tuple-element.22), kind=kOutput, calls=%fused_computation.5 | convolution fusion | flops 537395200 | bytes 3407872 | tf_op jit(solution)/shard_map/dot_general | solution.py:40
  53.0 1.7 %fusion = bf16[1,2048,256]{2,1,0:T(8,128)(2,1)} fusion(bf16[512,2048]{1,0:T(8,128)(2,1)S(1)} %bitcast.40, bf16[512,256]{1,0:T(8,128)(2,1)S(1)} %get-tuple-element.23), kind=kOutput, calls=%fused_computation.4 | convolution fusion | flops 537395200 | bytes 3407872 | tf_op jit(solution)/shard_map/dot_general | solution.py:37
  54.8 0.7 fusion.3
  55.5 0.0 copy-start.2
  55.5 0.7 add_convert_fusion
  56.3 0.5 copy-done.2
  56.8 0.0 copy-start.4
  56.8 0.0 copy-start.5
  56.8 0.0 copy-start.6
  56.8 0.0 copy-start.7
  56.8 0.0 copy-start.8
  56.8 0.0 copy-start.9
  56.8 36.8 %shard_map.189.tg = bf16[256,2048]{1,0:T(8,128)(2,1)S(1)} custom-call(bf16[8,64,2048]{2,1,0:T(8,128)(2,1)S(1)} %bitcast.34, bf16[256,2048]{1,0:T(8,128)(2,1)S(1)} %copy-done.2, s32[256,2]{1,0:T(8,128)S(1)} %copy.21.ids), custom_call_target="tpu_custom_call" | custom-call | tf_op jit(solution)/shard_map/pallas_call | solution.py:539
  93.6 0.0 copy-done.4
  93.6 0.0 copy-done.5
  93.6 0.0 copy-done.6
  93.6 0.0 copy-done.7
  93.6 0.0 copy-done.8
  93.6 0.0 copy-done.9
  93.7 33.7 %shard_map.190 = (bf16[256,128]{1,0:T(8,128)(2,1)S(1)}, bf16[256,128]{1,0:T(8,128)(2,1)S(1)}, bf16[256,256]{1,0:T(8,128)(2,1)S(1)}, f32[256,128]{1,0:T(8,128)S(1)}, f32[256,256]{1,0:T(8,128)S(1)}) custom-call(bf16[256,2048]{1,0:T(8,128)(2,1)S(1)} %shard_map.189.tg, bf16[2048,256]{1,0:T(8,128)(2,1)S(1)} %copy-done.4, bf16[256,256]{1,0:T(8,128)(2,1)S(1)} %copy-done.5, ...), custom_call_target="tpu_custom_call" | custom-call | flops 2000000000 | bytes 4000000 | tf_op jit(solution)/shard_map/pallas_call | solution.py:242
  127.3 0.7 copy.29
  128.0 0.6 copy.30
  128.7 0.6 copy.31
  129.3 0.7 copy.32
  130.0 0.7 copy.33
Async XLA Ops:
  0.6 45.6 %copy-start = (bf16[1,2048,256]{2,1,0:T(8,128)(2,1)S(1)}, bf16[1,2048,256]{2,1,0:T(8,128)(2,1)}, u32[]{:S(2)}) copy-start(bf16[1,2048,256]{2,1,0:T(8,128)(2,1)} %param.17) | copy-start | bytes 3145732
  2.4 1.2 copy-start.1
  3.6 1.2 copy-start.3
  46.2 1.2 copy-start.10
  47.4 1.2 copy-start.11
  55.5 1.2 copy-start.2
  56.8 36.8 %copy-start.4 = (bf16[2048,256]{1,0:T(8,128)(2,1)S(1)}, bf16[2048,256]{1,0:T(8,128)(2,1)}, u32[]{:S(2)}) copy-start(bf16[2048,256]{1,0:T(8,128)(2,1)} %ow.1) | copy-start | bytes 3145732
  56.8 36.8 %copy-start.5 = (bf16[256,256]{1,0:T(8,128)(2,1)S(1)}, bf16[256,256]{1,0:T(8,128)(2,1)}, u32[]{:S(2)}) copy-start(bf16[256,256]{1,0:T(8,128)(2,1)} %mo.1) | copy-start | bytes 393220
  56.8 36.9 %copy-start.6 = (bf16[256,256]{1,0:T(8,128)(2,1)S(1)}, bf16[256,256]{1,0:T(8,128)(2,1)}, u32[]{:S(2)}) copy-start(bf16[256,256]{1,0:T(8,128)(2,1)} %v.1) | copy-start | bytes 393220
  56.8 36.9 %copy-start.7 = (f32[256,128]{1,0:T(8,128)S(1)}, f32[256,128]{1,0:T(8,128)}, u32[]{:S(2)}) copy-start(f32[256,128]{1,0:T(8,128)} %a.1) | copy-start | bytes 393220
  56.8 36.9 %copy-start.8 = (bf16[256,128]{1,0:T(8,128)(2,1)S(1)}, bf16[256,128]{1,0:T(8,128)(2,1)}, u32[]{:S(2)}) copy-start(bf16[256,128]{1,0:T(8,128)(2,1)} %q.1) | copy-start | bytes 196612
  56.8 36.9 %copy-start.9 = (bf16[256,128]{1,0:T(8,128)(2,1)S(1)}, bf16[256,128]{1,0:T(8,128)(2,1)}, u32[]{:S(2)}) copy-start(bf16[256,128]{1,0:T(8,128)(2,1)} %k.1) | copy-start | bytes 196612
